TPU v7x, 128 devices: a whole 4x4x4 slice. The times are simulated.
128 devices in a mesh: sp: 16 (over z, x), tp: 8 (over y, core).
Axes of the slice: x: 4, y: 4, z: 4, core: 2. Of those that a mesh axis runs over, the one named last changes fastest.
Arguments:
- stream: bfloat16 [4096, 2048], P(('sp', 'tp')), may hold values from -5 to 5
- out_gate: bfloat16 [4096, 2048], P('sp', 'tp'), may hold values from -6 to 6
- in_gate: bfloat16 [4096, 2048], P('sp', 'tp'), may hold values from -6 to 6
- values: bfloat16 [4096, 2048], P('sp', 'tp'), may hold values from -6 to 6
- conv_weight: float32 [3, 2048], P(None, 'tp'), may hold values from -3 to 3
- out_weight: bfloat16 [2048, 2048], replicated, may hold values from -0.125 to 0.125
- doc_ids: int32 [4096], P('sp'), may hold values from 0 to 5, never falling along the last dimension, each value on 1 to 1024 neighbouring positions
- routes: int32 [4096, 2], P(('sp', 'tp')), may hold values from 0 to 15, all different within a row; in each aligned block of 32 rows (0 to 31, 32 to 63, ...) at most 5 rows name the same one
- route_weight: float32 [4096, 2], P(('sp', 'tp')), may hold values from 0.2 to 1
- norm_gain: float32 [2, 2048], replicated, may hold values from 0.1 to 1.9
- norm_bias: float32 [2, 2048], replicated, may hold values from -2 to 2
- expert_gate: bfloat16 [16, 2048, 7168], P('sp', None, 'tp'), may hold values from -0.125 to 0.125
- expert_up: bfloat16 [16, 2048, 7168], P('sp', None, 'tp'), may hold values from -0.125 to 0.125
- expert_down: bfloat16 [16, 7168, 2048], P('sp', 'tp'), may hold values from -0.0625 to 0.0625
Outputs:
- layer_out: bfloat16 [4096, 2048], P(('sp', 'tp'))
Inputs may be any that keep to these rules, and one draw needn't show every extreme that they name: `doc_ids`: each document occupies consecutive positions, numbers never fall along positions, each document has at most 1024 positions and one has exactly 1024. `routes`: each row names two different experts. In each aligned block of 32 rows (the rows of one device) no expert is named more than 5 times, a bound that some block reaches.
All inputs are finite; a program needn't handle non-finite values.
Results may differ from a plain program's by a relative error of at most 0.012.
Values may be sent and summed in bfloat16 or wider, within the bound.
A program may use at most 64 MiB of HBM per device.

v0:
```python
import jax
import jax.numpy as jnp
from jax import lax
from jax.sharding import PartitionSpec as P

TOK_DEV = 256


residual_scale = 1.6817928


def passed_along(value, axis, steps):
    count = lax.axis_size(axis)
    initial, last = (max(0, -steps), min(count, count - steps))
    return lax.ppermute(value, axis, [(source, source + steps) for source in range(initial, last)])


def in_order(parts, dim):
    shape = list(parts.shape[1:])
    shape[dim] *= parts.shape[0]
    return jnp.moveaxis(parts, 0, dim).reshape(shape)


def sent_to_all(array, axis):
    copies = jnp.broadcast_to(array, (lax.axis_size(axis), *array.shape))
    return lax.all_to_all(copies, axis, split_axis=0, concat_axis=0, tiled=True)


def gathered_copies(array, axis, dim):
    return in_order(sent_to_all(array, axis), dim)


def in_blocks(array, dim, count):
    before, after = (array.shape[:dim], array.shape[dim + 1 :])
    return jnp.moveaxis(array.reshape(*before, count, -1, *after), dim, 0)


def sent_and_summed(array, axis, dim):
    parts = in_blocks(array, dim, lax.axis_size(axis))
    arrived = lax.all_to_all(parts, axis, split_axis=0, concat_axis=0, tiled=True)
    return arrived.astype(jnp.float32).sum(axis=0)


def layer_norm(values_in, gain_row, bias_row):
    row_mean = jnp.mean(values_in, axis=-1, keepdims=True)
    centered = values_in - row_mean
    variance = jnp.mean(centered * centered, axis=-1, keepdims=True)
    return centered * lax.rsqrt(variance + 1e-05) * gain_row + bias_row


def shards(
    stream,
    out_gate,
    in_gate,
    values,
    conv_weight,
    out_weight,
    doc_ids,
    routes,
    route_weight,
    norm_gain,
    norm_bias,
    expert_gate,
    expert_up,
    expert_down,
):
    length = doc_ids.shape[0]
    model_width = out_weight.shape[1]
    gated_values = in_gate.astype(jnp.float32) * values.astype(jnp.float32)
    tail_rows, tail_docs = passed_along(
        (gated_values[length - 2 :], doc_ids[length - 2 :]), "sp", 1
    )
    extended = jnp.concatenate([tail_rows, gated_values], axis=0)
    ext_docs = jnp.concatenate([tail_docs, doc_ids], axis=0)
    keep_first = (ext_docs[1 : length + 1] == doc_ids).astype(jnp.float32)[:, None]
    keep_second = (ext_docs[0:length] == doc_ids).astype(jnp.float32)[:, None]
    convolved = (
        conv_weight[0] * extended[0:length] * keep_second
        + conv_weight[1] * extended[1 : length + 1] * keep_first
        + conv_weight[2] * gated_values
    )
    mixed_rows = (out_gate.astype(jnp.float32) * convolved).astype(jnp.bfloat16)
    token_rows = lax.all_to_all(mixed_rows, "tp", split_axis=0, concat_axis=1, tiled=True)
    projected = jnp.dot(token_rows, out_weight, preferred_element_type=jnp.float32)
    normed = layer_norm(
        residual_scale * stream.astype(jnp.float32) + projected, norm_gain[0], norm_bias[0]
    ).astype(jnp.bfloat16)
    experts = lax.axis_size("sp")
    groups = lax.axis_size("tp")
    capacity = max(2, 5 * TOK_DEV // (2 * groups * experts))
    row_count = normed.shape[0]
    expert_ids = routes.reshape(-1)
    onehot = (expert_ids[:, None] == jnp.arange(experts, dtype=jnp.int32)[None, :]).astype(
        jnp.int32
    )
    slot_rank = jnp.sum((jnp.cumsum(onehot, axis=0) - onehot) * onehot, axis=1)
    slot_index = expert_ids * capacity + slot_rank
    placement_map = (
        jnp.arange(experts * capacity, dtype=jnp.int32)[:, None] == slot_index[None, :]
    ).astype(jnp.bfloat16)
    repeated = jnp.repeat(normed, 2, axis=0)
    send_rows = jnp.dot(placement_map, repeated, preferred_element_type=jnp.float32).astype(
        jnp.bfloat16
    )
    send_rows = send_rows.reshape(experts, capacity, model_width)
    received = lax.all_to_all(send_rows, "sp", split_axis=0, concat_axis=0, tiled=True)
    grouped = gathered_copies(received[:, None], "tp", 1)
    flat_rows = grouped.reshape(experts * groups * capacity, model_width)
    gate_part = jnp.dot(flat_rows, expert_gate[0], preferred_element_type=jnp.float32)
    up_part = jnp.dot(flat_rows, expert_up[0], preferred_element_type=jnp.float32)
    hidden = (jax.nn.silu(gate_part) * up_part).astype(jnp.bfloat16)
    partial_value = jnp.dot(hidden, expert_down[0], preferred_element_type=jnp.float32)
    partial_value = partial_value.reshape(experts, groups, capacity, model_width)
    summed = sent_and_summed(partial_value.astype(jnp.bfloat16), "tp", 1)
    back_rows = summed.reshape(experts, capacity, model_width).astype(jnp.bfloat16)
    returned = lax.all_to_all(back_rows, "sp", split_axis=0, concat_axis=0, tiled=True)
    picked = jnp.take(returned.reshape(experts * capacity, model_width), slot_index, axis=0)
    picked = picked.astype(jnp.float32).reshape(row_count, 2, model_width)
    routed_sum = jnp.sum(picked * route_weight[:, :, None], axis=1)
    return layer_norm(
        residual_scale * normed.astype(jnp.float32) + routed_sum, norm_gain[1], norm_bias[1]
    ).astype(jnp.bfloat16)


def solution(mesh):
    in_specs = (
        P(("sp", "tp"), None),
        P("sp", "tp"),
        P("sp", "tp"),
        P("sp", "tp"),
        P(None, "tp"),
        P(),
        P("sp"),
        P(("sp", "tp"), None),
        P(("sp", "tp"), None),
        P(),
        P(),
        P("sp", None, "tp"),
        P("sp", None, "tp"),
        P("sp", "tp", None),
    )
    out_specs = P(("sp", "tp"), None)
    return jax.shard_map(shards, mesh=mesh, in_specs=in_specs, out_specs=out_specs, check_vma=False)
```

profile of v0, /device:TPU:0, one launch (start us, length us, event | category | flops | bytes accessed | tf_op | source)
XLA Modules:
  0.0 170.7 jit_solution(18152803575538419704)
XLA Ops:
  0.0 1.0 convert_multiply_fusion
  1.0 3.5 %collective-permute-start = (f32[2,256]{1,0:T(2,128)S(1)}, f32[2,256]{1,0:T(2,128)S(1)}, u32[]{:S(2)}, u32[]{:S(2)}) collective-permute-start(f32[2,256]{1,0:T(2,128)S(1)} %slice.54), channel_id=1, source_target_pairs={{0,8},{8,16},{16,24},{24,32},{32,40},{40,48},{48,56},{56,64},{64,7... | collective-permute-start | bytes 6152 | tf_op jit(solution)/shard_map/ppermute | solution.py:15
  5.3 3.4 %collective-permute-start.1 = (s32[2]{0:T(128)S(1)}, s32[2]{0:T(128)S(1)}, u32[]{:S(2)}, u32[]{:S(2)}) collective-permute-start(s32[2]{0:T(128)S(1)} %slice.42), channel_id=1, source_target_pairs={{0,8},{8,16},{16,24},{24,32},{32,40},{40,48},{48,56},{56,64},{64,7... | collective-permute-start | bytes 32 | tf_op jit(solution)/shard_map/ppermute | solution.py:15
  8.7 0.8 fusion.29
  13.9 1.7 %fusion.21 = bf16[256,256]{1,0:T(8,128)(2,1)} fusion(f32[2,256]{1,0:T(2,128)S(1)} %collective-permute-done, f32[256,256]{1,0:T(8,128)S(1)} %convert_multiply_fusion, bf16[256,256]{1,0:T(8,128)(2,1)} %param.15, f32[256]{0:T(256)S(1)} %bitcast.62, f32[256]{0:T(256)S(1)} %get-tuple-element.13, f32[256]{0:T(256)S(1)} %bitcast.63, f32[256]{0:T(256)S(1)} %get-tuple-element.12, ...), kind=kLoop, calls=%fused_computation.23 | loop fusion | flops 786432 | bytes 531456 | tf_op jit(solution)/shard_map/convert_element_type | solution.py:82
  15.6 4.5 %all-to-all-start = ((bf16[8,32,256]{2,1,0:T(8,128)(2,1)}), bf16[8,32,256]{2,1,0:T(8,128)(2,1)S(1)}, u32[]{:S(2)}, u32[]{:S(2)}) async-start(bf16[8,32,256]{2,1,0:T(8,128)(2,1)} %bitcast.3), calls=%async_computation | async-start | bytes 262144 | tf_op jit(solution)/shard_map/all_to_all | solution.py:83
  20.1 6.1 %all-to-all-done = bf16[8,32,256]{2,1,0:T(8,128)(2,1)S(1)} async-done(((bf16[8,32,256]{2,1,0:T(8,128)(2,1)}), bf16[8,32,256]{2,1,0:T(8,128)(2,1)S(1)}, u32[]{:S(2)}, u32[]{:S(2)}) %all-to-all-start) | async-done | bytes 131104 | tf_op jit(solution)/shard_map/all_to_all | solution.py:83
  26.2 5.0 %fusion.31 = (f32[32]{0:T(128)S(1)}, f32[32,2048]{1,0:T(8,128)S(1)}) fusion(bf16[32,2048]{1,0:T(8,128)(2,1)S(1)} %bitcast.49, bf16[2048,2048]{1,0:T(8,128)(2,1)} %param.19, bf16[32,2048]{1,0:T(8,128)(2,1)} %param.14), kind=kOutput, calls=%fused_computation.57 | convolution fusion | flops 268697568 | bytes 8913024 | tf_op jit(solution)/shard_map/dot_general | solution.py:84
  32.2 18.6 %all_to_all.39 = bf16[16,5,2048]{2,1,0:T(8,128)(2,1)S(1)} all-to-all(bf16[16,5,2048]{2,1,0:T(8,128)(2,1)S(1)} %reshape.103), channel_id=1, replica_groups=mesh['sp'=16,'tp'=8] {'sp'}, dimensions={0} | all-to-all | bytes 655360 | tf_op jit(solution)/shard_map/all_to_all | solution.py:106
  51.4 35.3 %all_to_all.40 = bf16[8,16,1,5,2048]{4,1,3,2,0:T(8,128)(2,1)S(1)} all-to-all(bf16[8,16,1,5,2048]{4,1,3,2,0:T(8,128)(2,1)S(1)} %broadcast_in_dim.16), channel_id=1, replica_groups=mesh['sp'=16,'tp'=8] {'tp'}, dimensions={0} | all-to-all | bytes 5242880 | tf_op jit(solution)/shard_map/all_to_all | solution.py:26
  86.7 3.4 %copy.63 = bf16[16,8,1,5,2048]{4,3,1,0,2:T(8,128)(2,1)} copy(bf16[16,8,1,5,2048]{4,0,3,2,1:T(8,128)(2,1)S(1)} %bitcast.48) | data formatting | bytes 5242880 | tf_op jit(solution)/shard_map/transpose | solution.py:21
  90.1 4.2 %reshape_reshape.3 = bf16[640,2048]{1,0:T(8,128)(2,1)S(1)} reshape(bf16[16,8,1,5,2048]{4,3,1,0,2:T(8,128)(2,1)} %copy.63) | data formatting | bytes 5242880 | tf_op jit(solution)/shard_map/reshape;reshape | solution.py:108
  94.3 5.1 %fusion.4 = f32[640,896]{1,0:T(8,128)S(1)} fusion(bf16[640,2048]{1,0:T(8,128)(2,1)S(1)} %reshape_reshape.3, bf16[1,2048,896]{2,1,0:T(8,128)(2,1)} %param.25), kind=kOutput, calls=%fused_computation.5 | convolution fusion | flops 2348810240 | bytes 8585216 | tf_op jit(solution)/shard_map/dot_general | solution.py:109
  99.4 4.0 %multiply_convert_fusion = bf16[640,896]{1,0:T(8,128)(2,1)} fusion(f32[640,896]{1,0:T(8,128)S(1)} %fusion.4, bf16[640,2048]{1,0:T(8,128)(2,1)S(1)} %reshape_reshape.3, bf16[1,2048,896]{2,1,0:T(8,128)(2,1)S(1)} %copy-done.2), kind=kOutput, calls=%fused_computation.10 | convolution fusion | flops 2352250880 | bytes 9732096 | tf_op jit(solution)/shard_map/dot_general | solution.py:110
  103.4 2.3 %dot_general.21 = bf16[16,8,5,896]{3,2,1,0:T(8,128)(2,1)S(1)} reshape(bf16[640,896]{1,0:T(8,128)(2,1)} %multiply_convert_fusion) | data formatting | bytes 2293760 | tf_op jit(solution)/shard_map/dot_general | solution.py:112
  105.7 5.1 %fusion.9 = bf16[8,16,1,5,2048]{4,0,3,1,2:T(8,128)(2,1)S(1)} fusion(bf16[1,896,2048]{2,1,0:T(8,128)(2,1)} %param.27, bf16[16,8,5,896]{3,2,1,0:T(8,128)(2,1)S(1)} %dot_general.21), kind=kOutput, calls=%fused_computation.8 | convolution fusion | flops 2350120960 | bytes 7438336 | tf_op jit(solution)/shard_map/dot_general | solution.py:112
  110.8 2.9 %copy.65 = bf16[8,16,1,5,2048]{4,1,3,2,0:T(8,128)(2,1)} copy(bf16[8,16,1,5,2048]{4,0,3,1,2:T(8,128)(2,1)S(1)} %fusion.9) | data formatting | bytes 5242880 | tf_op jit(solution)/shard_map/transpose | solution.py:35
  113.7 3.8 %all-to-all-start.3 = ((bf16[8,16,1,5,2048]{4,1,3,2,0:T(8,128)(2,1)}), bf16[8,16,1,5,2048]{4,1,3,2,0:T(8,128)(2,1)S(1)}, u32[]{:S(2)}, u32[]{:S(2)}) async-start(bf16[8,16,1,5,2048]{4,1,3,2,0:T(8,128)(2,1)} %copy.65), calls=%async_computation.3 | async-start | bytes 5242880 | tf_op jit(solution)/shard_map/all_to_all | solution.py:40
  118.1 32.1 %all-to-all-done.3 = bf16[8,16,1,5,2048]{4,1,3,2,0:T(8,128)(2,1)S(1)} async-done(((bf16[8,16,1,5,2048]{4,1,3,2,0:T(8,128)(2,1)}), bf16[8,16,1,5,2048]{4,1,3,2,0:T(8,128)(2,1)S(1)}, u32[]{:S(2)}, u32[]{:S(2)}) %all-to-all-start.3) | async-done | bytes 2621472 | tf_op jit(solution)/shard_map/all_to_all | solution.py:40
  150.7 1.0 copy.66
  151.7 3.6 %all-to-all-start.4 = ((bf16[16,5,2048]{2,1,0:T(8,128)(2,1)}), bf16[16,5,2048]{2,1,0:T(8,128)(2,1)S(1)}, u32[]{:S(2)}, u32[]{:S(2)}) async-start(bf16[16,5,2048]{2,1,0:T(8,128)(2,1)} %copy.66), calls=%async_computation.4 | async-start | bytes 1048576 | tf_op jit(solution)/shard_map/all_to_all | solution.py:116
  155.3 11.5 %all-to-all-done.4 = bf16[16,5,2048]{2,1,0:T(8,128)(2,1)S(1)} async-done(((bf16[16,5,2048]{2,1,0:T(8,128)(2,1)}), bf16[16,5,2048]{2,1,0:T(8,128)(2,1)S(1)}, u32[]{:S(2)}, u32[]{:S(2)}) %all-to-all-start.4) | async-done | bytes 327712 | tf_op jit(solution)/shard_map/all_to_all | solution.py:116
  167.8 1.5 multiply_reduce_fusion
  169.8 0.8 add_convert_fusion
  (49 shorter events, 9.3 us)
Async XLA Ops:
  1.0 12.8 %collective-permute-start = (f32[2,256]{1,0:T(2,128)S(1)}, f32[2,256]{1,0:T(2,128)S(1)}, u32[]{:S(2)}, u32[]{:S(2)}) collective-permute-start(f32[2,256]{1,0:T(2,128)S(1)} %slice.54), channel_id=1, source_target_pairs={{0,8},{8,16},{16,24},{24,32},{32,40},{40,48},{48,56},{56,64},{64,7... | collective-permute-start | bytes 6152 | tf_op jit(solution)/shard_map/ppermute | solution.py:15
  5.3 7.1 %collective-permute-start.1 = (s32[2]{0:T(128)S(1)}, s32[2]{0:T(128)S(1)}, u32[]{:S(2)}, u32[]{:S(2)}) collective-permute-start(s32[2]{0:T(128)S(1)} %slice.42), channel_id=1, source_target_pairs={{0,8},{8,16},{16,24},{24,32},{32,40},{40,48},{48,56},{56,64},{64,7... | collective-permute-start | bytes 32 | tf_op jit(solution)/shard_map/ppermute | solution.py:15
  15.6 10.6 %all-to-all-start = ((bf16[8,32,256]{2,1,0:T(8,128)(2,1)}), bf16[8,32,256]{2,1,0:T(8,128)(2,1)S(1)}, u32[]{:S(2)}, u32[]{:S(2)}) async-start(bf16[8,32,256]{2,1,0:T(8,128)(2,1)} %bitcast.3), calls=%async_computation | async-start | bytes 262144 | tf_op jit(solution)/shard_map/all_to_all | solution.py:83
  94.3 5.1 %copy-start.2 = (bf16[1,2048,896]{2,1,0:T(8,128)(2,1)S(1)}, bf16[1,2048,896]{2,1,0:T(8,128)(2,1)}, u32[]{:S(2)}) copy-start(bf16[1,2048,896]{2,1,0:T(8,128)(2,1)} %param.26) | copy-start | bytes 11010052
  113.7 3.9 %copy-start = (s32[32,2]{0,1:T(2,128)S(1)}, s32[32,2]{0,1:T(2,128)}, u32[]{:S(2)}) copy-start(s32[32,2]{0,1:T(2,128)} %param.21) | copy-start | bytes 772
  113.7 4.3 %copy-start.1 = (f32[32,2]{0,1:T(2,128)S(1)}, f32[32,2]{0,1:T(2,128)}, u32[]{:S(2)}) copy-start(f32[32,2]{0,1:T(2,128)} %param.22) | copy-start | bytes 772
  113.7 36.5 %all-to-all-start.3 = ((bf16[8,16,1,5,2048]{4,1,3,2,0:T(8,128)(2,1)}), bf16[8,16,1,5,2048]{4,1,3,2,0:T(8,128)(2,1)S(1)}, u32[]{:S(2)}, u32[]{:S(2)}) async-start(bf16[8,16,1,5,2048]{4,1,3,2,0:T(8,128)(2,1)} %copy.65), calls=%async_computation.3 | async-start | bytes 5242880 | tf_op jit(solution)/shard_map/all_to_all | solution.py:40
  151.7 15.1 %all-to-all-start.4 = ((bf16[16,5,2048]{2,1,0:T(8,128)(2,1)}), bf16[16,5,2048]{2,1,0:T(8,128)(2,1)S(1)}, u32[]{:S(2)}, u32[]{:S(2)}) async-start(bf16[16,5,2048]{2,1,0:T(8,128)(2,1)} %copy.66), calls=%async_computation.4 | async-start | bytes 1048576 | tf_op jit(solution)/shard_map/all_to_all | solution.py:116
where the time goes:
time: 172 us; the launch traced here: 171 us
  blocking collectives  53.9 us (31%)
  waiting for transfers between devices  49.7 us (29%)
  local copies, waits for them, and re-layouts  20.4 us (12%)
  matrix products  19.4 us (11%)
  starting transfers between devices  18.7 us (11%)
  other arithmetic  8.27 us (5%)
    all_to_all x1, blocking collectives, sent_to_all(): return lax.all_to_all(copies, axis, split_axis=0, concat_axis=0, tiled=True)  35.3 us
    all_to_all x1, waiting for transfers between devices, sent_and_summed(): lax.all_to_all(parts, axis, split_axis=0, concat_axis=0, tiled=True)  32.1 us
    all_to_all x1, blocking collectives, shards(): lax.all_to_all(send_rows, 'sp', split_axis=0, concat_axis=0, tiled=True)  18.6 us
    all_to_all x1, waiting for transfers between devices, shards(): lax.all_to_all(back_rows, 'sp', split_axis=0, concat_axis=0, tiled=True)  11.5 us
    ppermute x2, starting transfers between devices, passed_along(): lax.ppermute(value, axis, [(source, source + steps) for source in range(i...  6.89 us
    all_to_all x1, waiting for transfers between devices, shards(): lax.all_to_all(mixed_rows, 'tp', split_axis=0, concat_axis=1, tiled=True)  6.1 us
    dot_general x1, matrix products, shards(): jnp.dot(hidden, expert_down[0], preferred_element_type=jnp.float32)  5.13 us
    dot_general x1, matrix products, shards(): jnp.dot(flat_rows, expert_gate[0], preferred_element_type=jnp.float32)  5.05 us
  transfers between devices with their start and end apart: 5, of which 3 were waited for; matrix products, arithmetic and copies ran while one was open for 4% of the time, Pallas kernels for 0%

commit v1 on v0

v1 whole, which is shorter than its diff:
```python
import jax
import jax.numpy as jnp
from jax import lax
from jax.experimental import pallas as pl
from jax.experimental.pallas import tpu as pltpu
from jax.sharding import PartitionSpec as P

MESH = pl.DeviceIdType.MESH
RESIDUAL = 1.6817928
NX = 4
NZ = 4
NSP = 16
NTP = 8
CAP = 5
PAD = 8
NT = 4
F32 = jnp.float32
BF16 = jnp.bfloat16


def layer_norm(v, gain, bias):
    mean = jnp.mean(v, axis=-1, keepdims=True)
    cent = v - mean
    var = jnp.mean(cent * cent, axis=-1, keepdims=True)
    return cent * lax.rsqrt(var + 1e-05) * gain + bias


def one_hot(cond):
    return jnp.where(cond, 1.0, 0.0).astype(BF16)


def body(
    stream_h, og_h, ig_h, va_h, cw_h, ow_h, doc_h, rt_h, rw_h, ng_h, nb_h, wg_h, wu_h, wd_h,
    out_ref,
    stream, og, ig, va, cw, ow, doc, rt, rw, ng, nb, wg, wu, wd,
    ext, halo, mx, tr, acc, normed, snd, rcv, xb, hb, pf, pb, rd, q3, q1, q2, tq, ra, rb, snd2, ret,
    lsem, h_s, h_r, a_s, a_r, b_s, b_r, g_s, g_r, p_s, p_r, d_s, d_r, s3_s, s3_r, s2_s, s2_r, s1_s, s1_r, e_s, e_r,
):
    sp = lax.axis_index("sp")
    tp = lax.axis_index("tp")
    z, x = sp // NX, sp % NX
    y, c = tp // 2, tp % 2
    width = og.shape[1]
    length = og.shape[0]
    model = stream.shape[1]
    rows = stream.shape[0]
    hidden = wg.shape[1]
    blk = NSP * CAP
    tile = model // NT

    def sp_at(d):
        return ((z + d // NX) % NZ) * NX + (x + d % NX) % NX

    def sp_back(d):
        return ((z - d // NX + NZ) % NZ) * NX + (x - d % NX + NX) % NX

    def tp_at(o):
        return ((y + o // 2) % 4) * 2 + (c + o % 2) % 2

    def tp_from(o):
        return ((y - o // 2 + 4) % 4) * 2 + (c - o % 2 + 2) % 2

    def remote(src, dst, ss, rs, dev):
        return pltpu.make_async_remote_copy(
            src_ref=src, dst_ref=dst, send_sem=ss, recv_sem=rs, device_id=dev, device_id_type=MESH
        )

    barrier = pltpu.get_barrier_semaphore()
    for d in range(1, NSP):
        pl.semaphore_signal(barrier, inc=1, device_id=(sp_at(d), tp), device_id_type=MESH)
    for o in range(1, NTP):
        pl.semaphore_signal(barrier, inc=1, device_id=(sp, tp_at(o)), device_id_type=MESH)

    local = [
        pltpu.make_async_copy(src, dst, lsem.at[i])
        for i, (src, dst) in enumerate(
            [
                (ig_h, ig), (va_h, va), (cw_h, cw), (doc_h, doc), (og_h, og), (rt_h, rt), (rw_h, rw),
                (stream_h, stream), (ng_h, ng), (nb_h, nb), (ow_h, ow),
                (wg_h.at[0], wg), (wu_h.at[0], wu), (wd_h.at[0], wd),
            ]
        )
    ]
    for copy in local:
        copy.start()

    for i in range(4):
        local[i].wait()
    ext[8:8 + length, :width] = ig[...].astype(F32) * va[...].astype(F32)
    ext[8:8 + length, width:] = jnp.transpose(jnp.broadcast_to(doc[...].astype(F32), (128, length)))
    local[4].wait()
    pl.semaphore_wait(barrier, NSP - 1 + NTP - 1)
    nxt = (sp + 1) % NSP
    halo_copy = remote(ext.at[pl.ds(length, 8), :], halo, h_s, h_r, (nxt, tp))
    halo_copy.start()

    def mixed(r0, n):
        d0 = ext[8 + r0:8 + r0 + n, width:]
        keep1 = jnp.where(ext[7 + r0:7 + r0 + n, width:] == d0, 1.0, 0.0)
        keep2 = jnp.where(ext[6 + r0:6 + r0 + n, width:] == d0, 1.0, 0.0)
        keep1 = jnp.concatenate([keep1] * (width // 128), axis=1)
        keep2 = jnp.concatenate([keep2] * (width // 128), axis=1)
        conv = (
            cw[0:1, :] * ext[6 + r0:6 + r0 + n, :width] * keep2
            + cw[1:2, :] * ext[7 + r0:7 + r0 + n, :width] * keep1
            + cw[2:3, :] * ext[8 + r0:8 + r0 + n, :width]
        )
        return (og[r0:r0 + n, :].astype(F32) * conv).astype(BF16)

    for t in range(1, NTP):
        mx[t] = mixed(t * rows, rows)
    a_copies = [
        remote(mx.at[tp_at(o)], tr.at[o], a_s.at[o], a_r.at[o], (sp, tp_at(o))) for o in range(1, NTP)
    ]
    order = (4, 5, 2, 3, 6, 7, 1)
    for o in order:
        @pl.when(tp_at(o) != 0)
        def _():
            a_copies[o - 1].start()

    halo_copy.wait_recv()
    ext[0:8, :width] = halo[:, :width]
    ext[0:8, width:] = jnp.where(sp == 0, -1.0, halo[:, width:])
    mx[0] = mixed(0, rows)
    for o in order:
        @pl.when(tp_at(o) == 0)
        def _():
            a_copies[o - 1].start()

    local[5].wait()
    local[6].wait()

    def relative(k):
        e = rt[k:k + 1, :]
        return (((e >> 2) + (NZ - z)) & 3) * NX + (((e & 3) + (NX - x)) & 3)

    rel = [relative(0), relative(1)]
    lanes = lax.broadcasted_iota(jnp.int32, (NSP, rows), 0)
    hot = [jnp.where(lanes == r, 1.0, 0.0) for r in rel]
    upper = one_hot(
        lax.broadcasted_iota(jnp.int32, (rows, rows), 0) < lax.broadcasted_iota(jnp.int32, (rows, rows), 1)
    )
    prefix = jnp.dot((hot[0] + hot[1]).astype(BF16), upper, preferred_element_type=F32)
    slots = lax.broadcasted_iota(jnp.int32, (NSP * PAD, rows), 0)
    place = []
    for k in range(2):
        rank = jnp.sum(prefix * hot[k], axis=0, keepdims=True)
        slot = rel[k] * PAD + rank.astype(jnp.int32)
        place.append(jnp.where(slots == slot, 1.0, 0.0))

    for i in range(7, 11):
        local[i].wait()
    tr[0] = mx[tp]
    acc[...] = RESIDUAL * stream[...].astype(F32)

    def project(o, _):
        @pl.when(o > 0)
        def _():
            remote(mx.at[tp_at(o)], tr.at[o], a_s.at[o], a_r.at[o], (sp, tp_at(o))).wait_recv()

        start = pl.multiple_of(tp_from(o) * width, width)
        acc[...] += jnp.dot(tr[o], ow[pl.ds(start, width), :], preferred_element_type=F32)
        return 0

    lax.fori_loop(0, NTP, project, 0)
    normed[...] = layer_norm(acc[...], ng[0:1, :], nb[0:1, :]).astype(BF16)

    both = (place[0] + place[1]).astype(BF16)
    for n in range(NT):
        cols = slice(n * tile, (n + 1) * tile)
        packed = jnp.dot(both, normed[:, cols], preferred_element_type=F32)
        snd[:, :, cols] = packed.reshape(NSP, PAD, tile).astype(BF16)
    b_copies = {
        d: remote(snd.at[d], rcv.at[d], b_s.at[d], b_r.at[d], (sp_at(d), tp)) for d in range(1, NSP)
    }
    sp_order = (10, 9, 11, 6, 14, 5, 7, 13, 15, 2, 8, 1, 3, 4, 12)
    for d in sp_order:
        b_copies[d].start()
    rcv[0] = snd[0]
    for d in sp_order:
        b_copies[d].wait_recv()
    row_i = lax.broadcasted_iota(jnp.int32, (blk, NSP * PAD), 0)
    slot_i = lax.broadcasted_iota(jnp.int32, (blk, NSP * PAD), 1)
    squeeze = one_hot(slot_i == (row_i & (NSP - 1)) * PAD + (row_i >> 4))
    for n in range(NT):
        cols = slice(n * tile, (n + 1) * tile)
        padded = rcv[:, :, cols].astype(F32).reshape(NSP * PAD, tile).astype(BF16)
        xb[0:blk, cols] = jnp.dot(squeeze, padded, preferred_element_type=F32).astype(BF16)

    fdir = 1 - 2 * c
    up = (sp, ((y + fdir + 4) % 4) * 2 + c)
    down = (sp, ((y - fdir + 4) % 4) * 2 + c)
    mate = (sp, y * 2 + 1 - c)
    position = {0: 0, 4: 1, 1: 2, 2: 3, 5: 4, 6: 5, 3: 6, 7: 7}

    def block(j):
        return xb.at[pl.ds(position[j] * blk, blk), :]

    to_up = remote(block(0), block(1), g_s.at[0], g_r.at[0], up)
    to_down = remote(block(0), block(2), g_s.at[1], g_r.at[1], down)
    forward = remote(block(1), block(3), g_s.at[2], g_r.at[2], up)
    pair = [remote(block(j), block(4 + j), p_s.at[j], p_r.at[j], mate) for j in range(4)]
    to_up.start()
    to_down.start()
    pair[0].start()

    def gate_up(r0, m):
        def some(gw, uw):
            xs = xb[r0:r0 + m, :]
            gate = jnp.dot(xs, gw, preferred_element_type=F32)
            upp = jnp.dot(xs, uw, preferred_element_type=F32)
            return (gate / (1.0 + jnp.exp(-gate)) * upp).astype(BF16)

        full = hidden // 256

        def step(i, _):
            cols = pl.ds(pl.multiple_of(i * 256, 256), 256)
            hb[0:m, cols] = some(wg[:, cols], wu[:, cols])
            return 0

        lax.fori_loop(0, full, step, 0)
        if hidden % 256:
            cols = slice(full * 256, hidden)
            hb[0:m, cols] = some(wg[:, cols], wu[:, cols])

    def d2d(k, n):
        lo, size = ((0, 1), (1, 2), (3, 1))[k]
        view = (pl.ds(lo * blk, size * blk), pl.ds(n * tile, tile))
        return remote(pb.at[view], rd.at[view], d_s.at[k * NT + n], d_r.at[k * NT + n], mate)

    def down_tile(k, n):
        lo, size = ((0, 1), (1, 2), (3, 1))[k]
        cols = slice(n * tile, (n + 1) * tile)
        m = 2 * size * blk
        part = jnp.dot(hb[0:m, :], wd[:, cols], preferred_element_type=F32)
        pf[lo * blk:(lo + size) * blk, cols] = part[:size * blk]
        pb[lo * blk:(lo + size) * blk, cols] = part[size * blk:].astype(BF16)
        d2d(k, n).start()

    def cols_of(n):
        return (slice(None), pl.ds(n * tile, tile))

    def send3(n):
        return remote(q3.at[cols_of(n)], tq.at[cols_of(n)], s3_s.at[n], s3_r.at[n], down)

    def send2(n):
        return remote(q2.at[cols_of(n)], rb.at[cols_of(n)], s2_s.at[n], s2_r.at[n], up)

    def send1(n):
        return remote(q1.at[cols_of(n)], ra.at[cols_of(n)], s1_s.at[n], s1_r.at[n], down)

    def summed(j, n):
        cols = slice(n * tile, (n + 1) * tile)
        return pf[j * blk:(j + 1) * blk, cols] + rd[j * blk:(j + 1) * blk, cols].astype(F32)

    pair[0].wait_recv()
    local[11].wait()
    local[12].wait()
    gate_up(0, 2 * blk)
    local[13].wait()
    for n in range(NT):
        down_tile(0, n)

    to_up.wait_recv()
    forward.start()
    pair[1].start()
    to_down.wait_recv()
    pair[2].start()
    pair[1].wait_recv()
    pair[2].wait_recv()
    gate_up(2 * blk, 4 * blk)
    forward.wait_recv()
    pair[3].start()

    def finish2(n):
        d2d(1, n).wait_recv()
        q2[:, n * tile:(n + 1) * tile] = summed(2, n).astype(BF16)
        send2(n).start()

    for n in range(NT):
        down_tile(1, n)
        if n > 0:
            finish2(n - 1)
    finish2(NT - 1)

    pair[3].wait_recv()
    gate_up(6 * blk, 2 * blk)

    def finish3(n):
        d2d(2, n).wait_recv()
        q3[:, n * tile:(n + 1) * tile] = summed(3, n).astype(BF16)
        send3(n).start()

    for n in range(NT):
        down_tile(2, n)
        if n > 0:
            finish3(n - 1)
    finish3(NT - 1)
    for n in range(NT):
        send3(n).wait_recv()
        cols = slice(n * tile, (n + 1) * tile)
        q1[:, cols] = (summed(1, n) + tq[:, cols].astype(F32)).astype(BF16)
        send1(n).start()
    spread = one_hot(
        lax.broadcasted_iota(jnp.int32, (NSP * PAD, blk), 0)
        == (lax.broadcasted_iota(jnp.int32, (NSP * PAD, blk), 1) & (NSP - 1)) * PAD
        + (lax.broadcasted_iota(jnp.int32, (NSP * PAD, blk), 1) >> 4)
    )
    for n in range(NT):
        d2d(0, n).wait_recv()
        send2(n).wait_recv()
        send1(n).wait_recv()
        cols = slice(n * tile, (n + 1) * tile)
        total = (summed(0, n) + ra[:, cols].astype(F32) + rb[:, cols].astype(F32)).astype(BF16)
        wide = jnp.dot(spread, total, preferred_element_type=F32)
        snd2[:, :, cols] = wide.reshape(NSP, PAD, tile).astype(BF16)

    e_copies = {
        d: remote(snd2.at[d], ret.at[d], e_s.at[d], e_r.at[d], (sp_back(d), tp)) for d in range(1, NSP)
    }
    for d in sp_order:
        e_copies[d].start()
    ret[0] = snd2[0]
    eye = lax.broadcasted_iota(jnp.int32, (rows, rows), 0) == lax.broadcasted_iota(jnp.int32, (rows, rows), 1)
    weight = [
        jnp.sum(jnp.where(eye, rw[k:k + 1, :], 0.0), axis=1, keepdims=True) for k in range(2)
    ]
    place = [p.astype(BF16) for p in place]
    for d in sp_order:
        e_copies[d].wait_recv()
    for n in range(NT):
        cols = slice(n * tile, (n + 1) * tile)
        came = ret[:, :, cols].astype(F32).reshape(NSP * PAD, tile).astype(BF16)
        routed = [
            weight[k]
            * lax.dot_general(place[k], came, (((0,), (0,)), ((), ())), preferred_element_type=F32)
            for k in range(2)
        ]
        acc[:, cols] = RESIDUAL * normed[:, cols].astype(F32) + (routed[0] + routed[1])
    out_ref[...] = layer_norm(acc[...], ng[1:2, :], nb[1:2, :]).astype(BF16)

    halo_copy.wait_send()
    for copy in a_copies:
        copy.wait_send()
    for d in sp_order:
        b_copies[d].wait_send()
        e_copies[d].wait_send()
    for copy in (to_up, to_down, forward, *pair):
        copy.wait_send()
    for n in range(NT):
        for k in range(3):
            d2d(k, n).wait_send()
        send3(n).wait_send()
        send2(n).wait_send()
        send1(n).wait_send()


def shards(stream, out_gate, in_gate, values, conv_weight, out_weight, doc_ids, routes, route_weight,
           norm_gain, norm_bias, expert_gate, expert_up, expert_down):
    length, width = out_gate.shape
    rows, model = stream.shape
    hidden = expert_gate.shape[2]
    blk = NSP * CAP
    any_spec = pl.BlockSpec(memory_space=pl.ANY)
    dma = pltpu.SemaphoreType.DMA
    scratch = [
        pltpu.VMEM((rows, model), BF16),
        pltpu.VMEM((length, width), BF16),
        pltpu.VMEM((length, width), BF16),
        pltpu.VMEM((length, width), BF16),
        pltpu.VMEM((3, width), F32),
        pltpu.VMEM((model, model), BF16),
        pltpu.VMEM((1, length), jnp.int32),
        pltpu.VMEM((2, rows), jnp.int32),
        pltpu.VMEM((2, rows), F32),
        pltpu.VMEM((2, model), F32),
        pltpu.VMEM((2, model), F32),
        pltpu.VMEM((model, hidden), BF16),
        pltpu.VMEM((model, hidden), BF16),
        pltpu.VMEM((hidden, model), BF16),
        pltpu.VMEM((8 + length, width + 128), F32),
        pltpu.VMEM((8, width + 128), F32),
        pltpu.VMEM((NTP, rows, width), BF16),
        pltpu.VMEM((NTP, rows, width), BF16),
        pltpu.VMEM((rows, model), F32),
        pltpu.VMEM((rows, model), BF16),
        pltpu.VMEM((NSP, PAD, model), BF16),
        pltpu.VMEM((NSP, PAD, model), BF16),
        pltpu.VMEM((8 * blk, model), BF16),
        pltpu.VMEM((4 * blk, hidden), BF16),
        pltpu.VMEM((4 * blk, model), F32),
        pltpu.VMEM((4 * blk, model), BF16),
        pltpu.VMEM((4 * blk, model), BF16),
        pltpu.VMEM((blk, model), BF16),
        pltpu.VMEM((blk, model), BF16),
        pltpu.VMEM((blk, model), BF16),
        pltpu.VMEM((blk, model), BF16),
        pltpu.VMEM((blk, model), BF16),
        pltpu.VMEM((blk, model), BF16),
        pltpu.VMEM((NSP, PAD, model), BF16),
        pltpu.VMEM((NSP, PAD, model), BF16),
        dma((14,)), dma, dma, dma((NTP,)), dma((NTP,)), dma((NSP,)), dma((NSP,)),
        dma((3,)), dma((3,)), dma((4,)), dma((4,)), dma((3 * NT,)), dma((3 * NT,)),
        dma((NT,)), dma((NT,)), dma((NT,)), dma((NT,)), dma((NT,)), dma((NT,)),
        dma((NSP,)), dma((NSP,)),
    ]
    return pl.pallas_call(
        body,
        out_shape=jax.ShapeDtypeStruct((rows, model), BF16),
        in_specs=[any_spec] * 14,
        out_specs=pl.BlockSpec(memory_space=pltpu.VMEM),
        scratch_shapes=scratch,
        compiler_params=pltpu.CompilerParams(
            collective_id=0, has_side_effects=True, vmem_limit_bytes=60 * 1024 * 1024
        ),
        name="layer",
    )(
        stream, out_gate, in_gate, values, conv_weight, out_weight, doc_ids.reshape(1, -1),
        routes.T, route_weight.T, norm_gain, norm_bias, expert_gate, expert_up, expert_down,
    )


def solution(mesh):
    in_specs = (
        P(("sp", "tp"), None),
        P("sp", "tp"),
        P("sp", "tp"),
        P("sp", "tp"),
        P(None, "tp"),
        P(),
        P("sp"),
        P(("sp", "tp"), None),
        P(("sp", "tp"), None),
        P(),
        P(),
        P("sp", None, "tp"),
        P("sp", None, "tp"),
        P("sp", "tp", None),
    )
    out_specs = P(("sp", "tp"), None)
    return jax.shard_map(shards, mesh=mesh, in_specs=in_specs, out_specs=out_specs, check_vma=False)
```

time: 172 us -> 66.1 us (0.38)
  Pallas kernels: 0 us -> 63.6 us
  blocking collectives: 53.9 us -> 0 us
  waiting for transfers between devices: 49.7 us -> 0 us
  matrix products: 19.4 us -> 0 us
  local copies, waits for them, and re-layouts: 20.4 us -> 1.57 us
  starting transfers between devices: 18.7 us -> 0 us
  other arithmetic: 8.27 us -> 0 us
    pallas_call x0 -> x1, Pallas kernels: none -> 63.6 us  [shards(): pl.pallas_call(body, out_shape=jax.ShapeDtypeStruct((rows, model), BF16),...]
    all_to_all x2 -> x0, blocking collectives: 53.9 us -> none  [the longest x1 35.3 us: sent_to_all(): return lax.all_to_all(copies, axis, split_axis=0, concat_axis=0, tiled=True)]
    all_to_all x3 -> x0, waiting for transfers between devices: 49.7 us -> none  [the longest x1 32.1 us: sent_and_summed(): lax.all_to_all(parts, axis, split_axis=0, concat_axis=0, tiled=True)]
    dot_general x5 -> x0, matrix products: 19.4 us -> none  [the longest x1 5.13 us: shards(): jnp.dot(hidden, expert_down[0], preferred_element_type=jnp.float32)]
    all_to_all x3 -> x0, starting transfers between devices: 11.8 us -> none  [the longest x1 4.47 us: shards(): lax.all_to_all(mixed_rows, 'tp', split_axis=0, concat_axis=1, tiled=True)]
    ppermute x2 -> x0, starting transfers between devices: 6.89 us -> none  [passed_along(): lax.ppermute(value, axis, [(source, source + steps) for source in range(i...]
    transpose x2 -> x0, local copies, waits for them, and re-layouts: 6.36 us -> none  [the longest x1 3.42 us: in_order(): return jnp.moveaxis(parts, 0, dim).reshape(shape)]
    another operation x1 -> x0, local copies, waits for them, and re-layouts: 4.18 us -> none  [shards(): flat_rows = grouped.reshape(experts * groups * capacity, model_width)]
  transfers between devices with their start and end apart: 5 -> 0, of which waited for: 3 -> 0; matrix products, arithmetic and copies ran while one was open for 4% -> 0% of each run, Pallas kernels for 0% -> 0%
where the time goes in v1:
time: 66.1 us; the launch traced here: 65.2 us
  Pallas kernels  63.6 us (96%)
  local copies, waits for them, and re-layouts  1.57 us (2%)
    pallas_call x1, Pallas kernels, shards(): pl.pallas_call(body, out_shape=jax.ShapeDtypeStruct((rows, model), BF16),...  63.6 us
    unnamed x1, local copies, waits for them, and re-layouts  1.57 us

profile of v1, /device:TPU:0, one launch (start us, length us, event | category | flops | bytes accessed | tf_op | source)
XLA Modules:
  0.0 65.2 jit_solution(2772639081792335119)
XLA Ops:
  0.0 63.6 %layer.1 = bf16[32,2048]{1,0:T(8,128)(2,1)} custom-call(bf16[32,2048]{1,0:T(8,128)(2,1)} %stream_h.1, bf16[256,256]{1,0:T(8,128)(2,1)} %og_h.1, bf16[256,256]{1,0:T(8,128)(2,1)} %ig_h.1, bf16[256,256]{1,0:T(8,128)(2,1)} %va_h.1, f32[3,256]{1,0:T(4,128)} %cw_h.1, bf16[2048,2048]{1,0:T(8,128)(2,1)} %ow_h.1, s32[1,256]{1,0:T(1,128)} %bitcast.3, ...), custom_call_target="tpu_custom_call" | custom-call | tf_op jit(solution)/shard_map/layer/pallas_call | solution.py:407
  63.6 1.6 %copy.16 = bf16[32,2048]{1,0:T(8,128)(2,1)} copy(bf16[32,2048]{1,0:T(8,128)(2,1)} %layer.1) | data formatting | bytes 262144

commit v2 on v1

v2 whole, which is shorter than its diff:
```python
import jax
import jax.numpy as jnp
from jax import lax
from jax.experimental import pallas as pl
from jax.experimental.pallas import tpu as pltpu
from jax.sharding import PartitionSpec as P

MESH = pl.DeviceIdType.MESH
RESIDUAL = 1.6817928
NX = 4
NZ = 4
NSP = 16
NTP = 8
CAP = 5
LB = 8
NT = 4
LAG = 2
F32 = jnp.float32
BF16 = jnp.bfloat16


def layer_norm(v, gain, bias):
    mean = jnp.mean(v, axis=-1, keepdims=True)
    cent = v - mean
    var = jnp.mean(cent * cent, axis=-1, keepdims=True)
    return cent * lax.rsqrt(var + 1e-05) * gain + bias


def one_hot(cond):
    return jnp.where(cond, 1.0, 0.0).astype(BF16)


def body(
    stream_h, og_h, ig_h, va_h, cw_h, ow_h, doc_h, rt_h, rw_h, ng_h, nb_h, wg_h, wu_h, wd_h,
    out_ref,
    stream, og, ig, va, cw, ow, doc, rt, rw, ng, nb, wg, wu, wd,
    ext, edge, edges, first, firsts, mx, tr, acc, normed, snd, rcv, xb, hb, pf, pb, rd, q1, q2, ra, rb, snd2, ret,
    rt_o, rw_o, normed_o, snd_o, rcv_o, snd2_o, ret_o, part_o, part, turn,
    lsem, h_s, h_r, i_s, i_r, a_s, a_r, b_s, b_r, g_s, g_r, p_s, p_r, d_s, d_r, s2_s, s2_r, s1_s, s1_r, e_s, e_r,
    o_s, o_r, c_s, c_r, f_s, f_r,
):
    sp = lax.axis_index("sp")
    tp = lax.axis_index("tp")
    z, x = sp // NX, sp % NX
    y, c = tp // 2, tp % 2
    width = og.shape[1]
    length = og.shape[0]
    model = stream.shape[1]
    rows = stream.shape[0]
    hidden = wg.shape[1]
    blk = NSP * CAP
    tile = model // NT
    half = model // 2

    def sp_at(d):
        return ((z + d // NX) % NZ) * NX + (x + d % NX) % NX

    def sp_back(d):
        return ((z - d // NX + NZ) % NZ) * NX + (x - d % NX + NX) % NX

    def tp_at(o):
        return ((y + o // 2) % 4) * 2 + (c + o % 2) % 2

    def tp_from(o):
        return ((y - o // 2 + 4) % 4) * 2 + (c - o % 2 + 2) % 2

    def remote(src, dst, ss, rs, dev):
        return pltpu.make_async_remote_copy(
            src_ref=src, dst_ref=dst, send_sem=ss, recv_sem=rs, device_id=dev, device_id_type=MESH
        )

    barrier = pltpu.get_barrier_semaphore()
    for d in range(1, NSP):
        pl.semaphore_signal(barrier, inc=1, device_id=(sp_at(d), tp), device_id_type=MESH)
    for o in range(1, NTP):
        pl.semaphore_signal(barrier, inc=1, device_id=(sp, tp_at(o)), device_id_type=MESH)

    nxt = (sp + 1) % NSP
    prv = (sp + NSP - 1) % NSP

    @pl.when(tp != 0)
    def _():
        pl.semaphore_signal(barrier, inc=1, device_id=(nxt, 0), device_id_type=MESH)

    @pl.when(tp == 0)
    def _():
        for t in range(1, NTP):
            pl.semaphore_signal(barrier, inc=1, device_id=(prv, t), device_id_type=MESH)

    local = [
        pltpu.make_async_copy(src, dst, lsem.at[i])
        for i, (src, dst) in enumerate(
            [
                (ig_h, ig), (va_h, va), (cw_h, cw), (doc_h, doc), (og_h, og), (rt_h, rt), (rw_h, rw),
                (stream_h, stream), (ng_h, ng), (nb_h, nb), (ow_h, ow),
                (wg_h.at[0], wg), (wu_h.at[0], wu), (wd_h.at[0], wd),
            ]
        )
    ]
    for copy in local[:10]:
        copy.start()

    for i in range(4):
        local[i].wait()
    ext[0:8, :width] = jnp.zeros((8, width), F32)
    ext[0:8, width:] = jnp.full((8, 128), -1.0, F32)
    ext[8:8 + length, :width] = ig[...].astype(F32) * va[...].astype(F32)
    ext[8:8 + length, width:] = jnp.transpose(jnp.broadcast_to(doc[...].astype(F32), (128, length)))
    local[4].wait()
    local[10].start()
    tail = ext[length:length + 8, :width]
    edge[:, :width] = cw[0:1, :] * tail
    edge[:, width:2 * width] = cw[1:2, :] * tail
    edge[:, 2 * width:] = ext[length:length + 8, width:]

    @pl.when(tp != 0)
    def _():
        pl.semaphore_wait(barrier, NSP + NTP - 1)

    @pl.when(tp == 0)
    def _():
        pl.semaphore_wait(barrier, NSP + 2 * NTP - 3)

    halo_copy = remote(edge, edges.at[tp], h_s, h_r.at[tp], (nxt, 0))
    halo_copy.start()
    far = (sp, ((y + 2) % 4) * 2 + c)
    local[5].wait()
    local[6].wait()
    far_copies = [
        remote(src, dst, o_s.at[i], o_r.at[i], far)
        for i, (src, dst) in enumerate([(rt, rt_o), (rw, rw_o), (normed, normed_o), (part_o, part)])
    ]
    far_copies[0].start()
    far_copies[1].start()

    def convolved(r0, n):
        d0 = ext[8 + r0:8 + r0 + n, width:]
        keep1 = jnp.where(ext[7 + r0:7 + r0 + n, width:] == d0, 1.0, 0.0)
        keep2 = jnp.where(ext[6 + r0:6 + r0 + n, width:] == d0, 1.0, 0.0)
        keep1 = jnp.concatenate([keep1] * (width // 128), axis=1)
        keep2 = jnp.concatenate([keep2] * (width // 128), axis=1)
        return (
            cw[0:1, :] * ext[6 + r0:6 + r0 + n, :width] * keep2
            + cw[1:2, :] * ext[7 + r0:7 + r0 + n, :width] * keep1
            + cw[2:3, :] * ext[8 + r0:8 + r0 + n, :width]
        )

    first[:, :width] = og[0:8, :].astype(F32)
    first[:, width:] = convolved(0, 8)

    @pl.when(tp != 0)
    def _():
        remote(first, firsts.at[tp], i_s, i_r.at[tp], (sp, 0)).start()

    for t in range(NTP):
        mx[t] = (og[t * rows:(t + 1) * rows, :].astype(F32) * convolved(t * rows, rows)).astype(BF16)
    a_copies = [
        remote(mx.at[tp_at(o)], tr.at[o], a_s.at[o], a_r.at[o], (sp, tp_at(o))) for o in range(1, NTP)
    ]
    for o in (4, 5, 2, 3, 6, 7, 1):
        a_copies[o - 1].start()
    for copy in local[11:]:
        copy.start()

    lanes = lax.broadcasted_iota(jnp.int32, (NSP, rows), 0)
    upper = one_hot(
        lax.broadcasted_iota(jnp.int32, (rows, rows), 0) < lax.broadcasted_iota(jnp.int32, (rows, rows), 1)
    )
    slots = lax.broadcasted_iota(jnp.int32, (blk, rows), 0)
    eye = lax.broadcasted_iota(jnp.int32, (rows, rows), 0) == lax.broadcasted_iota(jnp.int32, (rows, rows), 1)

    def placed(table):
        rel = []
        for k in range(2):
            e = table[k:k + 1, :]
            rel.append((((e >> 2) + (NZ - z)) & 3) * NX + (((e & 3) + (NX - x)) & 3))
        hot = [jnp.where(lanes == r, 1.0, 0.0) for r in rel]
        prefix = jnp.dot((hot[0] + hot[1]).astype(BF16), upper, preferred_element_type=F32)
        place = []
        for k in range(2):
            rank = jnp.sum(prefix * hot[k], axis=0, keepdims=True)
            slot = rel[k] * CAP + rank.astype(jnp.int32)
            place.append(jnp.where(slots == slot, 1.0, 0.0))
        return place

    def weights(table):
        return [jnp.sum(jnp.where(eye, table[k:k + 1, :], 0.0), axis=1, keepdims=True) for k in range(2)]

    place = placed(rt)

    for i in range(7, 11):
        local[i].wait()
    tr[0] = mx[tp]
    acc[...] = RESIDUAL * stream[...].astype(F32)

    def arrive(o):
        remote(mx.at[tp_at(o)], tr.at[o], a_s.at[o], a_r.at[o], (sp, tp_at(o))).wait_recv()

    @pl.when(tp == 0)
    def _():
        firsts[0] = first[...]
        row = lax.broadcasted_iota(jnp.int32, (8, 128), 0)
        d0 = ext[8:16, width:]
        for o in range(NTP):
            if o > 0:
                arrive(o)
        for o in range(NTP):
            t = tp_from(o)
            if o > 0:
                remote(first, firsts.at[t], i_s, i_r.at[t], (sp, 0)).wait_recv()
            remote(edge, edges.at[t], h_s, h_r.at[t], (nxt, 0)).wait_recv()
            came = pltpu.roll(edges[t], 2, 0)
            near = pltpu.roll(edges[t], 1, 0)
            live = jnp.where(sp > 0, 1.0, 0.0)
            keep2 = jnp.where((came[:, 2 * width:] == d0) & (row < 2), live, 0.0)
            keep1 = jnp.where((near[:, 2 * width:] == d0) & (row < 1), live, 0.0)
            keep2 = jnp.concatenate([keep2] * (width // 128), axis=1)
            keep1 = jnp.concatenate([keep1] * (width // 128), axis=1)
            conv = firsts[t, :, width:] + came[:, :width] * keep2 + near[:, width:2 * width] * keep1
            tr[o, 0:8, :] = (firsts[t, :, :width] * conv).astype(BF16)

    def project(o, _):
        @pl.when((o > 0) & (tp != 0))
        def _():
            arrive(o)

        start = pl.multiple_of(tp_from(o) * width, width)
        acc[...] += jnp.dot(tr[o], ow[pl.ds(start, width), :], preferred_element_type=F32)
        return 0

    lax.fori_loop(0, NTP, project, 0)
    normed[...] = layer_norm(acc[...], ng[0:1, :], nb[0:1, :]).astype(BF16)

    far_copies[2].start()

    def fold(rows_f32, dst, h):
        for b in range(LB):
            turn[pl.ds(b, blk, stride=LB), :] = rows_f32[:, b * 128:(b + 1) * 128]
        dst[h] = turn[...].reshape(NSP, CAP * LB, 128).astype(BF16)

    def unfold(src, h):
        turn[...] = src[h].astype(F32).reshape(blk * LB, 128)
        return jnp.concatenate(
            [turn[pl.ds(b, blk, stride=LB), :].astype(BF16) for b in range(LB)], axis=1
        )

    def pack(place, src, dst, h):
        both = (place[0] + place[1]).astype(BF16)
        fold(jnp.dot(both, src[:, h * half:(h + 1) * half], preferred_element_type=F32), dst, h)

    def halves(src, dst, ss, rs, to):
        return [
            {
                d: remote(
                    src.at[h, d], dst.at[h, d],
                    ss.at[h * NSP + d], rs.at[h * NSP + d], (to(d), tp),
                )
                for d in range(1, NSP)
            }
            for h in range(2)
        ]

    sp_order = (10, 9, 11, 6, 14, 5, 7, 13, 15, 2, 8, 1, 3, 4, 12)
    b_copies = halves(snd, rcv, b_s, b_r, sp_at)
    c_copies = halves(snd_o, rcv_o, c_s, c_r, sp_at)
    e_copies = halves(snd2, ret, e_s, e_r, sp_back)
    f_copies = halves(snd2_o, ret_o, f_s, f_r, sp_back)

    def start_all(copies):
        for d in sp_order:
            copies[d].start()

    def arrive_all(copies):
        for d in sp_order:
            copies[d].wait_recv()

    for h in range(2):
        pack(place, normed, snd, h)
        start_all(b_copies[h])
        rcv[h, 0] = snd[h, 0]
    far_copies[0].wait_recv()
    far_copies[1].wait_recv()
    place_o = placed(rt_o)
    fdir = 1 - 2 * c
    up = (sp, ((y + fdir + 4) % 4) * 2 + c)
    down = (sp, ((y - fdir + 4) % 4) * 2 + c)
    mate = (sp, y * 2 + 1 - c)
    position = {0: 0, 4: 1, 1: 2, 2: 3, 5: 4, 6: 5, 3: 6, 7: 7}

    def settle(src, j, h):
        r0 = position[j] * blk
        xb[h, r0:r0 + blk, :] = unfold(src, h)

    def block(j, h):
        return xb.at[h, pl.ds(position[j] * blk, blk), :]

    to_up = [remote(block(0, h), block(1, h), g_s.at[h], g_r.at[h], up) for h in range(2)]
    to_down = [remote(block(0, h), block(2, h), g_s.at[2 + h], g_r.at[2 + h], down) for h in range(2)]
    pair = [
        [remote(block(j, h), block(4 + j, h), p_s.at[2 * j + h], p_r.at[2 * j + h], mate) for h in range(2)]
        for j in range(4)
    ]

    def gather_half(h):
        arrive_all(b_copies[h])
        settle(rcv, 0, h)
        pair[0][h].start()
        to_up[h].start()
        to_down[h].start()

    gather_half(0)
    far_copies[2].wait_recv()
    for h in range(2):
        pack(place_o, normed_o, snd_o, h)
        start_all(c_copies[h])
        rcv_o[h, 0] = snd_o[h, 0]
    gather_half(1)

    def gate_up(r0, m):
        def some(gw, uw):
            lo, hi = xb[0, r0:r0 + m, :], xb[1, r0:r0 + m, :]
            gate, upp = [
                jnp.dot(lo, w[:half], preferred_element_type=F32)
                + jnp.dot(hi, w[half:], preferred_element_type=F32)
                for w in (gw, uw)
            ]
            return (gate / (1.0 + jnp.exp(-gate)) * upp).astype(BF16)

        full = hidden // 256

        def step(i, _):
            cols = pl.ds(pl.multiple_of(i * 256, 256), 256)
            hb[0:m, cols] = some(wg[:, cols], wu[:, cols])
            return 0

        lax.fori_loop(0, full, step, 0, unroll=True)
        if hidden % 256:
            cols = slice(full * 256, hidden)
            hb[0:m, cols] = some(wg[:, cols], wu[:, cols])

    def d2d(k, n):
        lo, size = ((0, 1), (1, 2), (3, 1))[k]
        view = (n, pl.ds(lo * blk, size * blk))
        return remote(pb.at[view], rd.at[view], d_s.at[k * NT + n], d_r.at[k * NT + n], mate)

    def down_tile(k, n):
        lo, size = ((0, 1), (1, 2), (3, 1))[k]
        cols = slice(n * tile, (n + 1) * tile)
        m = 2 * size * blk
        part = jnp.dot(hb[0:m, :], wd[:, cols], preferred_element_type=F32)
        pf[n, lo * blk:(lo + size) * blk, :] = part[:size * blk]
        pb[n, lo * blk:(lo + size) * blk, :] = part[size * blk:].astype(BF16)
        d2d(k, n).start()

    def send2(n):
        return remote(q2.at[n], rb.at[n], s2_s.at[n], s2_r.at[n], up)

    def send1(n):
        return remote(q1.at[n], ra.at[n], s1_s.at[n], s1_r.at[n], down)

    def summed(j, n):
        return pf[n, j * blk:(j + 1) * blk, :] + rd[n, j * blk:(j + 1) * blk, :].astype(F32)

    pair[0][0].wait_recv()
    pair[0][1].wait_recv()
    local[11].wait()
    local[12].wait()
    gate_up(0, 2 * blk)
    local[13].wait()
    for n in range(NT):
        down_tile(0, n)

    for h in range(2):
        arrive_all(c_copies[h])
        settle(rcv_o, 3, h)
        pair[3][h].start()

    def pass_on(h):
        to_up[h].wait_recv()
        pair[1][h].start()
        to_down[h].wait_recv()
        pair[2][h].start()

    pass_on(0)
    pair[3][0].wait_recv()
    pair[3][1].wait_recv()
    gate_up(6 * blk, 2 * blk)
    pass_on(1)

    for n in range(NT):
        down_tile(2, n)
    for h in range(2):
        pair[1][h].wait_recv()
        pair[2][h].wait_recv()
    gate_up(2 * blk, 4 * blk)

    def finish2(n):
        d2d(1, n).wait_recv()
        q1[n] = summed(1, n).astype(BF16)
        send1(n).start()
        q2[n] = summed(2, n).astype(BF16)
        send2(n).start()

    for n in range(NT):
        down_tile(1, n)
        if n >= LAG:
            finish2(n - LAG)
    for n in range(NT - LAG, NT):
        finish2(n)
    per = NT // 2
    for h in range(2):
        sums = []
        for n in range(h * per, (h + 1) * per):
            d2d(2, n).wait_recv()
            sums.append(summed(3, n))
        fold(jnp.concatenate(sums, axis=1), snd2_o, h)
        start_all(f_copies[h])
        ret_o[h, 0] = snd2_o[h, 0]

    for h in range(2):
        sums = []
        for n in range(h * per, (h + 1) * per):
            d2d(0, n).wait_recv()
            send2(n).wait_recv()
            send1(n).wait_recv()
            sums.append(summed(0, n) + ra[n].astype(F32) + rb[n].astype(F32))
        fold(jnp.concatenate(sums, axis=1), snd2, h)
        start_all(e_copies[h])
        ret[h, 0] = snd2[h, 0]

    def picked(place, weight, src, h):
        came = unfold(src, h)
        routed = [
            weight[k] * lax.dot_general(
                place[k].astype(BF16), came, (((0,), (0,)), ((), ())), preferred_element_type=F32
            )
            for k in range(2)
        ]
        return routed[0] + routed[1]

    weight_o = weights(rw_o)
    weight = weights(rw)
    for h in range(2):
        arrive_all(f_copies[h])
        part_o[:, h * half:(h + 1) * half] = picked(place_o, weight_o, ret_o, h).astype(BF16)
    far_copies[3].start()
    for h in range(2):
        cols = slice(h * half, (h + 1) * half)
        arrive_all(e_copies[h])
        acc[:, cols] = RESIDUAL * normed[:, cols].astype(F32) + picked(place, weight, ret, h)
    far_copies[3].wait_recv()
    acc[...] += part[...].astype(F32)
    out_ref[...] = layer_norm(acc[...], ng[1:2, :], nb[1:2, :]).astype(BF16)

    halo_copy.wait_send()

    @pl.when(tp != 0)
    def _():
        remote(first, firsts.at[tp], i_s, i_r.at[tp], (sp, 0)).wait_send()

    for copy in (*a_copies, *far_copies, *to_up, *to_down, *pair[0], *pair[1], *pair[2], *pair[3]):
        copy.wait_send()
    for d in sp_order:
        for h in range(2):
            for copies in (b_copies, c_copies, e_copies, f_copies):
                copies[h][d].wait_send()
    for n in range(NT):
        for k in range(3):
            d2d(k, n).wait_send()
        send2(n).wait_send()
        send1(n).wait_send()


def shards(stream, out_gate, in_gate, values, conv_weight, out_weight, doc_ids, routes, route_weight,
           norm_gain, norm_bias, expert_gate, expert_up, expert_down):
    length, width = out_gate.shape
    rows, model = stream.shape
    hidden = expert_gate.shape[2]
    blk = NSP * CAP
    any_spec = pl.BlockSpec(memory_space=pltpu.HBM)
    dma = pltpu.SemaphoreType.DMA
    scratch = [
        pltpu.VMEM((rows, model), BF16),
        pltpu.VMEM((length, width), BF16),
        pltpu.VMEM((length, width), BF16),
        pltpu.VMEM((length, width), BF16),
        pltpu.VMEM((3, width), F32),
        pltpu.VMEM((model, model), BF16),
        pltpu.VMEM((1, length), jnp.int32),
        pltpu.VMEM((2, rows), jnp.int32),
        pltpu.VMEM((2, rows), F32),
        pltpu.VMEM((2, model), F32),
        pltpu.VMEM((2, model), F32),
        pltpu.VMEM((model, hidden), BF16),
        pltpu.VMEM((model, hidden), BF16),
        pltpu.VMEM((hidden, model), BF16),
        pltpu.VMEM((8 + length, width + 128), F32),
        pltpu.VMEM((8, 2 * width + 128), F32),
        pltpu.VMEM((NTP, 8, 2 * width + 128), F32),
        pltpu.VMEM((8, 2 * width), F32),
        pltpu.VMEM((NTP, 8, 2 * width), F32),
        pltpu.VMEM((NTP, rows, width), BF16),
        pltpu.VMEM((NTP, rows, width), BF16),
        pltpu.VMEM((rows, model), F32),
        pltpu.VMEM((rows, model), BF16),
        pltpu.VMEM((2, NSP, CAP * LB, 128), BF16),
        pltpu.VMEM((2, NSP, CAP * LB, 128), BF16),
        pltpu.VMEM((2, 8 * blk, model // 2), BF16),
        pltpu.VMEM((4 * blk, hidden), BF16),
        pltpu.VMEM((NT, 4 * blk, model // NT), F32),
        pltpu.VMEM((NT, 4 * blk, model // NT), BF16),
        pltpu.VMEM((NT, 4 * blk, model // NT), BF16),
        pltpu.VMEM((NT, blk, model // NT), BF16),
        pltpu.VMEM((NT, blk, model // NT), BF16),
        pltpu.VMEM((NT, blk, model // NT), BF16),
        pltpu.VMEM((NT, blk, model // NT), BF16),
        pltpu.VMEM((2, NSP, CAP * LB, 128), BF16),
        pltpu.VMEM((2, NSP, CAP * LB, 128), BF16),
        pltpu.VMEM((2, rows), jnp.int32),
        pltpu.VMEM((2, rows), F32),
        pltpu.VMEM((rows, model), BF16),
        pltpu.VMEM((2, NSP, CAP * LB, 128), BF16),
        pltpu.VMEM((2, NSP, CAP * LB, 128), BF16),
        pltpu.VMEM((2, NSP, CAP * LB, 128), BF16),
        pltpu.VMEM((2, NSP, CAP * LB, 128), BF16),
        pltpu.VMEM((rows, model), BF16),
        pltpu.VMEM((rows, model), BF16),
        pltpu.VMEM((blk * LB, 128), F32),
        dma((14,)), dma, dma((NTP,)), dma, dma((NTP,)), dma((NTP,)), dma((NTP,)), dma((2 * NSP,)), dma((2 * NSP,)),
        dma((4,)), dma((4,)), dma((8,)), dma((8,)), dma((3 * NT,)), dma((3 * NT,)),
        dma((NT,)), dma((NT,)), dma((NT,)), dma((NT,)),
        dma((2 * NSP,)), dma((2 * NSP,)),
        dma((4,)), dma((4,)), dma((2 * NSP,)), dma((2 * NSP,)), dma((2 * NSP,)), dma((2 * NSP,)),
    ]
    return pl.pallas_call(
        body,
        out_shape=jax.ShapeDtypeStruct((rows, model), BF16),
        in_specs=[any_spec] * 14,
        out_specs=pl.BlockSpec(memory_space=pltpu.VMEM),
        scratch_shapes=scratch,
        compiler_params=pltpu.CompilerParams(
            collective_id=0, has_side_effects=True, vmem_limit_bytes=48 * 1024 * 1024
        ),
        name="layer",
    )(*[pltpu.with_memory_space_constraint(v, pltpu.HBM) for v in (
        stream, out_gate, in_gate, values, conv_weight, out_weight, doc_ids.reshape(1, -1),
        routes.T, route_weight.T, norm_gain, norm_bias, expert_gate, expert_up, expert_down,
    )])


def solution(mesh):
    in_specs = (
        P(("sp", "tp"), None),
        P("sp", "tp"),
        P("sp", "tp"),
        P("sp", "tp"),
        P(None, "tp"),
        P(),
        P("sp"),
        P(("sp", "tp"), None),
        P(("sp", "tp"), None),
        P(),
        P(),
        P("sp", None, "tp"),
        P("sp", None, "tp"),
        P("sp", "tp", None),
    )
    out_specs = P(("sp", "tp"), None)
    return jax.shard_map(shards, mesh=mesh, in_specs=in_specs, out_specs=out_specs, check_vma=False)
```

time: 66.1 us -> 54.6 us (0.83)
  Pallas kernels: 63.6 us -> 53.5 us
  local copies, waits for them, and re-layouts: 1.57 us -> 0.66 us
    pallas_call x1, Pallas kernels: 63.6 us -> 53.5 us  [shards(): pl.pallas_call(body, out_shape=jax.ShapeDtypeStruct((rows, model), BF16),...]
    unnamed x1, local copies, waits for them, and re-layouts: 1.57 us -> 0.66 us
where the time goes in v2:
time: 54.6 us; the launch traced here: 54.2 us
  Pallas kernels  53.5 us (98%)
  local copies, waits for them, and re-layouts  0.66 us (1%)
    pallas_call x1, Pallas kernels, shards(): pl.pallas_call(body, out_shape=jax.ShapeDtypeStruct((rows, model), BF16),...  53.5 us

profile of v2, /device:TPU:0, one launch (start us, length us, event | category | flops | bytes accessed | tf_op | source)
XLA Modules:
  0.0 54.2 jit_solution(11207593154784315706)
XLA Ops:
  0.0 53.5 %layer.1 = bf16[32,2048]{1,0:T(8,128)(2,1)S(1)} custom-call(bf16[32,2048]{1,0:T(8,128)(2,1)} %stream_h.1, bf16[256,256]{1,0:T(8,128)(2,1)} %og_h.1, bf16[256,256]{1,0:T(8,128)(2,1)} %ig_h.1, bf16[256,256]{1,0:T(8,128)(2,1)} %va_h.1, f32[3,256]{1,0:T(4,128)} %cw_h.1, bf16[2048,2048]{1,0:T(8,128)(2,1)} %ow_h.1, s32[1,256]{1,0:T(1,128)} %bitcast.3, ...), custom_call_target="tpu_custom_call" | custom-call | tf_op jit(solution)/shard_map/layer/pallas_call | solution.py:535
  53.5 0.7 %copy.16 = bf16[32,2048]{1,0:T(8,128)(2,1)} copy(bf16[32,2048]{1,0:T(8,128)(2,1)S(1)} %layer.1) | data formatting | bytes 262144

commit v3 on v2

v3 whole, which is shorter than its diff:
```python
import jax
import jax.numpy as jnp
from jax import lax
from jax.experimental import pallas as pl
from jax.experimental.pallas import tpu as pltpu
from jax.sharding import PartitionSpec as P

MESH = pl.DeviceIdType.MESH
RESIDUAL = 1.6817928
NX = 4
NZ = 4
NSP = 16
NTP = 8
CAP = 5
LB = 8
NT = 4
F32 = jnp.float32
BF16 = jnp.bfloat16


def layer_norm(v, gain, bias):
    mean = jnp.mean(v, axis=-1, keepdims=True)
    cent = v - mean
    var = jnp.mean(cent * cent, axis=-1, keepdims=True)
    return cent * lax.rsqrt(var + 1e-05) * gain + bias


def one_hot(cond):
    return jnp.where(cond, 1.0, 0.0).astype(BF16)


def body(
    stream_h, og_h, ig_h, va_h, cw_h, ow_h, doc_h, rt_h, rw_h, ng_h, nb_h, wg_h, wu_h, wd_h,
    out_ref,
    stream, og, ig, va, cw, ow, doc, rt, rw, ng, nb, wg, wu, wd,
    ext, halo, term, terms, mx, tr, acc, normed, snd, rcv, xb, hb, pf, pb, rd, q, rab, snd2, ret,
    rt_o, rw_o, normed_o, snd_o, rcv_o, snd2_o, ret_o, part_o, part, turn,
    lsem, h_s, h_r, i_s, i_r, a_s, a_r, b_s, b_r, g_s, g_r, p_s, p_r, d_s, d_r, q_s, q_r, e_s, e_r,
    o_s, o_r, c_s, c_r, f_s, f_r,
):
    sp = lax.axis_index("sp")
    tp = lax.axis_index("tp")
    z, x = sp // NX, sp % NX
    y, c = tp // 2, tp % 2
    width = og.shape[1]
    length = og.shape[0]
    model = stream.shape[1]
    rows = stream.shape[0]
    hidden = wg.shape[1]
    blk = NSP * CAP
    tile = model // NT
    half = model // 2
    per = NT // 2

    def sp_at(d):
        return ((z + d // NX) % NZ) * NX + (x + d % NX) % NX

    def sp_back(d):
        return ((z - d // NX + NZ) % NZ) * NX + (x - d % NX + NX) % NX

    def tp_at(o):
        return ((y + o // 2) % 4) * 2 + (c + o % 2) % 2

    def tp_from(o):
        return ((y - o // 2 + 4) % 4) * 2 + (c - o % 2 + 2) % 2

    def remote(src, dst, ss, rs, dev):
        return pltpu.make_async_remote_copy(
            src_ref=src, dst_ref=dst, send_sem=ss, recv_sem=rs, device_id=dev, device_id_type=MESH
        )

    def whole(ref, sem):
        remote(ref, ref, sem, sem, (sp, tp)).wait_recv()

    barrier = pltpu.get_barrier_semaphore()
    for d in range(1, NSP):
        pl.semaphore_signal(barrier, inc=1, device_id=(sp_at(d), tp), device_id_type=MESH)
    for o in range(1, NTP):
        pl.semaphore_signal(barrier, inc=1, device_id=(sp, tp_at(o)), device_id_type=MESH)

    nxt = (sp + 1) % NSP

    local = [
        pltpu.make_async_copy(src, dst, lsem.at[i])
        for i, (src, dst) in enumerate(
            [
                (ig_h, ig), (va_h, va), (cw_h, cw), (doc_h, doc), (og_h, og), (rt_h, rt), (rw_h, rw),
                (stream_h, stream), (ng_h, ng), (nb_h, nb), (ow_h, ow),
                (wg_h.at[0], wg), (wu_h.at[0], wu), (wd_h.at[0], wd),
            ]
        )
    ]
    for copy in local[:10]:
        copy.start()

    for i in range(4):
        local[i].wait()
    ext[0:8, :width] = jnp.zeros((8, width), F32)
    ext[0:8, width:] = jnp.full((8, 128), -1.0, F32)
    ext[8:8 + length, :width] = ig[...].astype(F32) * va[...].astype(F32)
    ext[8:8 + length, width:] = jnp.transpose(jnp.broadcast_to(doc[...].astype(F32), (128, length)))
    local[4].wait()
    local[10].start()
    pl.semaphore_wait(barrier, NSP + NTP - 2)
    halo_copy = remote(ext.at[pl.ds(length, 8), :], halo, h_s, h_r, (nxt, tp))
    halo_copy.start()
    far = (sp, ((y + 2) % 4) * 2 + c)
    local[5].wait()
    local[6].wait()
    far_copies = [
        remote(src, dst, o_s.at[i], o_r.at[i], far)
        for i, (src, dst) in enumerate([
            (rt, rt_o), (rw, rw_o),
            (normed.at[:, pl.ds(0, half)], normed_o.at[:, pl.ds(0, half)]),
            (normed.at[:, pl.ds(half, half)], normed_o.at[:, pl.ds(half, half)]),
            (part_o, part),
        ])
    ]
    far_copies[0].start()
    far_copies[1].start()

    def convolved(r0, n):
        d0 = ext[8 + r0:8 + r0 + n, width:]
        keep1 = jnp.where(ext[7 + r0:7 + r0 + n, width:] == d0, 1.0, 0.0)
        keep2 = jnp.where(ext[6 + r0:6 + r0 + n, width:] == d0, 1.0, 0.0)
        keep1 = jnp.concatenate([keep1] * (width // 128), axis=1)
        keep2 = jnp.concatenate([keep2] * (width // 128), axis=1)
        return (
            cw[0:1, :] * ext[6 + r0:6 + r0 + n, :width] * keep2
            + cw[1:2, :] * ext[7 + r0:7 + r0 + n, :width] * keep1
            + cw[2:3, :] * ext[8 + r0:8 + r0 + n, :width]
        )

    for t in range(NTP):
        mx[t] = (og[t * rows:(t + 1) * rows, :].astype(F32) * convolved(t * rows, rows)).astype(BF16)
    a_copies = [
        remote(mx.at[tp_at(o)], tr.at[o], a_s, a_r.at[o], (sp, tp_at(o))) for o in range(1, NTP)
    ]
    for o in (4, 5, 2, 3, 6, 7, 1):
        a_copies[o - 1].start()
    for copy in local[11:]:
        copy.start()

    lanes = lax.broadcasted_iota(jnp.int32, (NSP, rows), 0)
    upper = one_hot(
        lax.broadcasted_iota(jnp.int32, (rows, rows), 0) < lax.broadcasted_iota(jnp.int32, (rows, rows), 1)
    )
    slots = lax.broadcasted_iota(jnp.int32, (blk, rows), 0)
    eye = lax.broadcasted_iota(jnp.int32, (rows, rows), 0) == lax.broadcasted_iota(jnp.int32, (rows, rows), 1)

    def placed(table):
        rel = []
        for k in range(2):
            e = table[k:k + 1, :]
            rel.append((((e >> 2) + (NZ - z)) & 3) * NX + (((e & 3) + (NX - x)) & 3))
        hot = [jnp.where(lanes == r, 1.0, 0.0) for r in rel]
        prefix = jnp.dot((hot[0] + hot[1]).astype(BF16), upper, preferred_element_type=F32)
        place = []
        for k in range(2):
            rank = jnp.sum(prefix * hot[k], axis=0, keepdims=True)
            slot = rel[k] * CAP + rank.astype(jnp.int32)
            place.append(jnp.where(slots == slot, 1.0, 0.0))
        return place

    def weights(table):
        return [jnp.sum(jnp.where(eye, table[k:k + 1, :], 0.0), axis=1, keepdims=True) for k in range(2)]

    place = placed(rt)

    for i in range(7, 11):
        local[i].wait()

    def project(lhs, t):
        start = pl.multiple_of(t * width, width)
        return jnp.dot(lhs, ow[pl.ds(start, width), :], preferred_element_type=F32)

    acc[...] = RESIDUAL * stream[...].astype(F32) + project(mx[tp], tp)
    halo_copy.wait_recv()
    ext[0:8, :width] = halo[:, :width]
    ext[0:8, width:] = jnp.where(sp == 0, -1.0, halo[:, width:])
    fixed = (og[0:16, :].astype(F32) * convolved(0, 16)).astype(BF16)
    term[...] = project(fixed, tp)[0:2, :]

    @pl.when(tp != 0)
    def _():
        remote(term, terms.at[tp], i_s, i_r, (sp, 0)).start()

    for o in (1, 2, 3, 6, 7, 4, 5):
        a_copies[o - 1].wait_recv()
        acc[...] += project(tr[o], tp_from(o))

    @pl.when(tp == 0)
    def _():
        whole(terms.at[pl.ds(1, NTP - 1)], i_r)
        total = term[...]
        for t in range(1, NTP):
            total += terms[t]
        acc[0:2, :] = RESIDUAL * stream[0:2, :].astype(F32) + total

    normed[...] = layer_norm(acc[...], ng[0:1, :], nb[0:1, :]).astype(BF16)

    far_copies[2].start()
    far_copies[3].start()

    def fold(rows_f32, dst, h):
        for b in range(LB):
            turn[pl.ds(b, blk, stride=LB), :] = rows_f32[:, b * 128:(b + 1) * 128]
        dst[h] = turn[...].reshape(NSP, CAP * LB, 128).astype(BF16)

    def unfold(src, h):
        turn[...] = src[h].astype(F32).reshape(blk * LB, 128)
        return jnp.concatenate(
            [turn[pl.ds(b, blk, stride=LB), :].astype(BF16) for b in range(LB)], axis=1
        )

    def pack(place, src, dst, h):
        both = (place[0] + place[1]).astype(BF16)
        fold(jnp.dot(both, src[:, h * half:(h + 1) * half], preferred_element_type=F32), dst, h)

    def halves(src, dst, ss, rs, to):
        return [
            {
                d: remote(src.at[h, d], dst.at[h, d], ss, rs.at[h], (to(d), tp))
                for d in range(1, NSP)
            }
            for h in range(2)
        ]

    sp_order = (10, 9, 11, 6, 14, 5, 7, 13, 15, 2, 8, 1, 3, 4, 12)
    b_copies = halves(snd, rcv, b_s, b_r, sp_at)
    c_copies = halves(snd_o, rcv_o, c_s, c_r, sp_at)
    e_copies = halves(snd2, ret, e_s, e_r, sp_back)
    f_copies = halves(snd2_o, ret_o, f_s, f_r, sp_back)

    def start_all(copies):
        for d in sp_order:
            copies[d].start()

    def arrive_all(dst, rs, h):
        whole(dst.at[h, pl.ds(1, NSP - 1)], rs.at[h])

    for h in range(2):
        pack(place, normed, snd, h)
        start_all(b_copies[h])
        rcv[h, 0] = snd[h, 0]
    far_copies[0].wait_recv()
    far_copies[1].wait_recv()
    place_o = placed(rt_o)
    def side_of(row):
        return (1 - 2 * c) * (1 - 2 * (row // 3))

    side = side_of(y)
    above, below = (y + 1) % 4, (y + 3) % 4
    first_above = side_of(above) == -1
    first_below = side_of(below) == 1
    toward = [(sp, ((y + side + 4) % 4) * 2 + c), (sp, ((y - side + 4) % 4) * 2 + c)]
    mate = (sp, y * 2 + 1 - c)
    position = {0: 0, 4: 1, 3: 2, 7: 3, 1: 4, 5: 5, 2: 6, 6: 7}

    def settle(src, j, h):
        r0 = position[j] * blk
        xb[h, r0:r0 + blk, :] = unfold(src, h)

    def block(j, h):
        return xb.at[h, pl.ds(position[j] * blk, blk), :]

    def neighbour(row, is_first, h):
        k = jnp.where(is_first, 0, 1)
        rows_at = pl.multiple_of((position[1] + k * (position[2] - position[1])) * blk, blk)
        return remote(
            block(0, h), xb.at[h, pl.ds(rows_at, blk), :], g_s, g_r.at[2 * k + h], (sp, row * 2 + c)
        )

    to_near = [
        (first_above, [neighbour(above, first_above, h) for h in range(2)]),
        (first_below, [neighbour(below, first_below, h) for h in range(2)]),
    ]

    def from_near(j, h):
        remote(block(0, h), block(j, h), g_s, g_r.at[2 * (j - 1) + h], mate).wait_recv()

    pair = [
        [remote(block(j, h), block(4 + j, h), p_s, p_r.at[j], mate) for h in range(2)]
        for j in range(4)
    ]

    def gather_half(h):
        arrive_all(rcv, b_r, h)
        settle(rcv, 0, h)
        pair[0][h].start()
        for is_first, copies in to_near:
            @pl.when(is_first)
            def _():
                copies[h].start()

    def far_dispatch():
        for h in range(2):
            far_copies[2 + h].wait_recv()
            pack(place_o, normed_o, snd_o, h)
            start_all(c_copies[h])
            rcv_o[h, 0] = snd_o[h, 0]

    pl.when(tp == 0)(far_dispatch)
    gather_half(0)
    pl.when((tp != 0) & (tp != 4))(far_dispatch)
    gather_half(1)
    pl.when(tp == 4)(far_dispatch)

    def gate_up(j, between=()):
        r0 = position[j] * blk
        lo, hi = (xb.at[h, pl.ds(r0, 2 * blk), :] for h in range(2))
        for i, c0 in enumerate(range(0, hidden, 256)):
            cols = slice(c0, min(c0 + 256, hidden))
            gate, upp = [
                jnp.dot(lo[...], w[:half, cols], preferred_element_type=F32)
                + jnp.dot(hi[...], w[half:, cols], preferred_element_type=F32)
                for w in (wg, wu)
            ]
            hb[:, cols] = (gate / (1.0 + jnp.exp(-gate)) * upp).astype(BF16)
            if i < len(between) and between[i]:
                between[i]()

    def d2d(j, n):
        view = (n, pl.ds(j * blk, blk))
        return remote(pb.at[view], rd.at[view], d_s, d_r.at[2 * j + n // per], mate)

    def d2d_in(j, h):
        whole(rd.at[pl.ds(h * per, per), pl.ds(j * blk, blk)], d_r.at[2 * j + h])

    def pair_in(j):
        whole(xb.at[:, pl.ds(position[4 + j] * blk, blk)], p_r.at[j])

    def down_tiles(j, tiles):
        for n in tiles:
            part = jnp.dot(hb[...], wd[:, n * tile:(n + 1) * tile], preferred_element_type=F32)
            pf[n, j * blk:(j + 1) * blk, :] = part[:blk]
            pb[n, j * blk:(j + 1) * blk, :] = part[blk:].astype(BF16)
        for n in tiles:
            d2d(j, n).start()

    behind = (1 + side) // 2

    def send(j, n):
        k = behind if j == 1 else 1 - behind
        return remote(q.at[j - 1, n], rab.at[k, n], q_s, q_r.at[2 * k + n // per], toward[j - 1])

    def summed(j, n):
        return pf[n, j * blk:(j + 1) * blk, :] + rd[n, j * blk:(j + 1) * blk, :].astype(F32)

    def finish(j, h):
        d2d_in(j, h)
        for n in range(h * per, (h + 1) * per):
            q[j - 1, n] = summed(j, n).astype(BF16)
            send(j, n).start()

    def far_total(h):
        d2d_in(3, h)
        fold(jnp.concatenate([summed(3, n) for n in range(h * per, (h + 1) * per)], axis=1), snd2_o, h)
        start_all(f_copies[h])
        ret_o[h, 0] = snd2_o[h, 0]

    def down_pass(j):
        down_tiles(j, range(per))
        down_tiles(j, range(per, NT))

    local[11].wait()
    local[12].wait()
    local[13].wait()
    @pl.when(y != 0)
    def _():
        pair_in(0)
        gate_up(0)

    from_near(1, 0)
    pair[1][0].start()
    from_near(1, 1)
    pair[1][1].start()
    for is_first, copies in to_near:
        @pl.when(jnp.logical_not(is_first))
        def _():
            copies[0].start()
            copies[1].start()
    @pl.when(y != 0)
    def _():
        down_tiles(0, range(NT))

    for h in range(2):
        arrive_all(rcv_o, c_r, h)
        settle(rcv_o, 3, h)
        pair[3][h].start()
    pair_in(1)
    gate_up(1)
    down_pass(1)
    pair_in(3)
    gate_up(3, (None, lambda: finish(1, 0), lambda: finish(1, 1)))
    for h in range(2):
        from_near(2, h)
        pair[2][h].start()
    down_pass(3)
    pair_in(2)
    gate_up(2, (None, lambda: far_total(0), lambda: far_total(1)))
    down_pass(2)
    @pl.when(y == 0)
    def _():
        pair_in(0)
        gate_up(0, (None, lambda: finish(2, 0), lambda: finish(2, 1)))
        down_pass(0)

    @pl.when(y != 0)
    def _():
        finish(2, 0)
        finish(2, 1)

    def picked(place, weight, src, h):
        came = unfold(src, h)
        routed = [
            weight[k] * lax.dot_general(
                place[k].astype(BF16), came, (((0,), (0,)), ((), ())), preferred_element_type=F32
            )
            for k in range(2)
        ]
        return routed[0] + routed[1]

    weight_o = weights(rw_o)
    weight = weights(rw)

    def own_total(h):
        d2d_in(0, h)
        for k in range(2):
            whole(rab.at[k, pl.ds(h * per, per)], q_r.at[2 * k + h])
        sums = [
            summed(0, n) + rab[0, n].astype(F32) + rab[1, n].astype(F32)
            for n in range(h * per, (h + 1) * per)
        ]
        fold(jnp.concatenate(sums, axis=1), snd2, h)
        start_all(e_copies[h])
        ret[h, 0] = snd2[h, 0]

    own_total(0)
    for h in range(2):
        arrive_all(ret_o, f_r, h)
        part_o[:, h * half:(h + 1) * half] = picked(place_o, weight_o, ret_o, h).astype(BF16)
    far_copies[4].start()
    own_total(1)
    halo_copy.wait_send()

    @pl.when(tp != 0)
    def _():
        remote(term, terms.at[tp], i_s, i_r, (sp, 0)).wait_send()

    for copy in far_copies[:4]:
        copy.wait_send()
    whole(mx.at[pl.ds(1, NTP - 1)], a_s)
    for src, ss in ((snd, b_s), (snd_o, c_s), (snd2_o, f_s)):
        whole(src.at[:, pl.ds(1, NSP - 1)], ss)
    whole(xb.at[0, pl.ds(0, 4 * blk)], g_s)
    whole(xb.at[0], p_s)
    whole(pb, d_s)
    whole(q, q_s)
    for h in range(2):
        cols = slice(h * half, (h + 1) * half)
        arrive_all(ret, e_r, h)
        acc[:, cols] = RESIDUAL * normed[:, cols].astype(F32) + picked(place, weight, ret, h)
    far_copies[4].wait_recv()
    acc[...] += part[...].astype(F32)
    out_ref[...] = layer_norm(acc[...], ng[1:2, :], nb[1:2, :]).astype(BF16)

    far_copies[4].wait_send()
    whole(snd2.at[:, pl.ds(1, NSP - 1)], e_s)


def shards(stream, out_gate, in_gate, values, conv_weight, out_weight, doc_ids, routes, route_weight,
           norm_gain, norm_bias, expert_gate, expert_up, expert_down):
    length, width = out_gate.shape
    rows, model = stream.shape
    hidden = expert_gate.shape[2]
    blk = NSP * CAP
    any_spec = pl.BlockSpec(memory_space=pltpu.HBM)
    dma = pltpu.SemaphoreType.DMA
    scratch = [
        pltpu.VMEM((rows, model), BF16),
        pltpu.VMEM((length, width), BF16),
        pltpu.VMEM((length, width), BF16),
        pltpu.VMEM((length, width), BF16),
        pltpu.VMEM((3, width), F32),
        pltpu.VMEM((model, model), BF16),
        pltpu.VMEM((1, length), jnp.int32),
        pltpu.VMEM((2, rows), jnp.int32),
        pltpu.VMEM((2, rows), F32),
        pltpu.VMEM((2, model), F32),
        pltpu.VMEM((2, model), F32),
        pltpu.VMEM((model, hidden), BF16),
        pltpu.VMEM((model, hidden), BF16),
        pltpu.VMEM((hidden, model), BF16),
        pltpu.VMEM((8 + length, width + 128), F32),
        pltpu.VMEM((8, width + 128), F32),
        pltpu.VMEM((2, model), F32),
        pltpu.VMEM((NTP, 2, model), F32),
        pltpu.VMEM((NTP, rows, width), BF16),
        pltpu.VMEM((NTP, rows, width), BF16),
        pltpu.VMEM((rows, model), F32),
        pltpu.VMEM((rows, model), BF16),
        pltpu.VMEM((2, NSP, CAP * LB, 128), BF16),
        pltpu.VMEM((2, NSP, CAP * LB, 128), BF16),
        pltpu.VMEM((2, 8 * blk, model // 2), BF16),
        pltpu.VMEM((2 * blk, hidden), BF16),
        pltpu.VMEM((NT, 4 * blk, model // NT), F32),
        pltpu.VMEM((NT, 4 * blk, model // NT), BF16),
        pltpu.VMEM((NT, 4 * blk, model // NT), BF16),
        pltpu.VMEM((2, NT, blk, model // NT), BF16),
        pltpu.VMEM((2, NT, blk, model // NT), BF16),
        pltpu.VMEM((2, NSP, CAP * LB, 128), BF16),
        pltpu.VMEM((2, NSP, CAP * LB, 128), BF16),
        pltpu.VMEM((2, rows), jnp.int32),
        pltpu.VMEM((2, rows), F32),
        pltpu.VMEM((rows, model), BF16),
        pltpu.VMEM((2, NSP, CAP * LB, 128), BF16),
        pltpu.VMEM((2, NSP, CAP * LB, 128), BF16),
        pltpu.VMEM((2, NSP, CAP * LB, 128), BF16),
        pltpu.VMEM((2, NSP, CAP * LB, 128), BF16),
        pltpu.VMEM((rows, model), BF16),
        pltpu.VMEM((rows, model), BF16),
        pltpu.VMEM((blk * LB, 128), F32),
        dma((14,)), dma, dma, dma, dma, dma, dma((NTP,)), dma, dma((2,)),
        dma, dma((4,)), dma, dma((4,)), dma, dma((8,)),
        dma, dma((4,)), dma, dma((2,)),
        dma((5,)), dma((5,)), dma, dma((2,)), dma, dma((2,)),
    ]
    return pl.pallas_call(
        body,
        out_shape=jax.ShapeDtypeStruct((rows, model), BF16),
        in_specs=[any_spec] * 14,
        out_specs=pl.BlockSpec(memory_space=pltpu.VMEM),
        scratch_shapes=scratch,
        compiler_params=pltpu.CompilerParams(
            collective_id=0, has_side_effects=True, vmem_limit_bytes=48 * 1024 * 1024
        ),
        name="layer",
    )(*[pltpu.with_memory_space_constraint(v, pltpu.HBM) for v in (
        stream, out_gate, in_gate, values, conv_weight, out_weight, doc_ids.reshape(1, -1),
        routes.T, route_weight.T, norm_gain, norm_bias, expert_gate, expert_up, expert_down,
    )])


def solution(mesh):
    in_specs = (
        P(("sp", "tp"), None),
        P("sp", "tp"),
        P("sp", "tp"),
        P("sp", "tp"),
        P(None, "tp"),
        P(),
        P("sp"),
        P(("sp", "tp"), None),
        P(("sp", "tp"), None),
        P(),
        P(),
        P("sp", None, "tp"),
        P("sp", None, "tp"),
        P("sp", "tp", None),
    )
    out_specs = P(("sp", "tp"), None)
    return jax.shard_map(shards, mesh=mesh, in_specs=in_specs, out_specs=out_specs, check_vma=False)
```

time: 54.6 us -> 49.6 us (0.908)
  Pallas kernels: 53.5 us -> 48.8 us
    pallas_call x1, Pallas kernels: 53.5 us -> 48.8 us  [shards(): pl.pallas_call(body, out_shape=jax.ShapeDtypeStruct((rows, model), BF16),...]
where the time goes in v3:
time: 49.6 us; the launch traced here: 49.4 us
  Pallas kernels  48.8 us (98%)
  local copies, waits for them, and re-layouts  0.66 us (1%)
    pallas_call x1, Pallas kernels, shards(): pl.pallas_call(body, out_shape=jax.ShapeDtypeStruct((rows, model), BF16),...  48.8 us

profile of v3, /device:TPU:0, one launch (start us, length us, event | category | flops | bytes accessed | tf_op | source)
XLA Modules:
  0.0 49.4 jit_solution(5394556966784922688)
XLA Ops:
  0.0 48.8 %layer.1 = bf16[32,2048]{1,0:T(8,128)(2,1)S(1)} custom-call(bf16[32,2048]{1,0:T(8,128)(2,1)} %stream_h.1, bf16[256,256]{1,0:T(8,128)(2,1)} %og_h.1, bf16[256,256]{1,0:T(8,128)(2,1)} %ig_h.1, bf16[256,256]{1,0:T(8,128)(2,1)} %va_h.1, f32[3,256]{1,0:T(4,128)} %cw_h.1, bf16[2048,2048]{1,0:T(8,128)(2,1)} %ow_h.1, s32[1,256]{1,0:T(1,128)} %bitcast.3, ...), custom_call_target="tpu_custom_call" | custom-call | tf_op jit(solution)/shard_map/layer/pallas_call | solution.py:529
  48.8 0.7 %copy.16 = bf16[32,2048]{1,0:T(8,128)(2,1)} copy(bf16[32,2048]{1,0:T(8,128)(2,1)S(1)} %layer.1) | data formatting | bytes 262144

commit v4 on v3

--- a/solution.py
+++ b/solution.py
@@ -113,7 +113,8 @@
             (rt, rt_o), (rw, rw_o),
             (normed.at[:, pl.ds(0, half)], normed_o.at[:, pl.ds(0, half)]),
             (normed.at[:, pl.ds(half, half)], normed_o.at[:, pl.ds(half, half)]),
-            (part_o, part),
+            (part_o.at[:, pl.ds(0, half)], part.at[:, pl.ds(0, half)]),
+            (part_o.at[:, pl.ds(half, half)], part.at[:, pl.ds(half, half)]),
         ])
     ]
     far_copies[0].start()
@@ -175,20 +176,21 @@
         return jnp.dot(lhs, ow[pl.ds(start, width), :], preferred_element_type=F32)
 
     acc[...] = RESIDUAL * stream[...].astype(F32) + project(mx[tp], tp)
-    halo_copy.wait_recv()
-    ext[0:8, :width] = halo[:, :width]
-    ext[0:8, width:] = jnp.where(sp == 0, -1.0, halo[:, width:])
-    fixed = (og[0:16, :].astype(F32) * convolved(0, 16)).astype(BF16)
-    term[...] = project(fixed, tp)[0:2, :]
-
-    @pl.when(tp != 0)
-    def _():
-        remote(term, terms.at[tp], i_s, i_r, (sp, 0)).start()
-
+    def edge_rows():
+        halo_copy.wait_recv()
+        ext[0:8, :width] = halo[:, :width]
+        ext[0:8, width:] = jnp.where(sp == 0, -1.0, halo[:, width:])
+        fixed = (og[0:16, :].astype(F32) * convolved(0, 16)).astype(BF16)
+        term[...] = project(fixed, tp)[0:2, :]
+
+        @pl.when(tp != 0)
+        def _():
+            remote(term, terms.at[tp], i_s, i_r, (sp, 0)).start()
+
+    edge_rows()
     for o in (1, 2, 3, 6, 7, 4, 5):
         a_copies[o - 1].wait_recv()
         acc[...] += project(tr[o], tp_from(o))
-
     @pl.when(tp == 0)
     def _():
         whole(terms.at[pl.ds(1, NTP - 1)], i_r)
@@ -306,19 +308,20 @@
     gather_half(1)
     pl.when(tp == 4)(far_dispatch)
 
-    def gate_up(j, between=()):
+    def gate_up(j, beside={}):
         r0 = position[j] * blk
         lo, hi = (xb.at[h, pl.ds(r0, 2 * blk), :] for h in range(2))
         for i, c0 in enumerate(range(0, hidden, 256)):
             cols = slice(c0, min(c0 + 256, hidden))
+            start = beside[i]() if i in beside else None
             gate, upp = [
                 jnp.dot(lo[...], w[:half, cols], preferred_element_type=F32)
                 + jnp.dot(hi[...], w[half:, cols], preferred_element_type=F32)
                 for w in (wg, wu)
             ]
             hb[:, cols] = (gate / (1.0 + jnp.exp(-gate)) * upp).astype(BF16)
-            if i < len(between) and between[i]:
-                between[i]()
+            if start:
+                start()
 
     def d2d(j, n):
         view = (n, pl.ds(j * blk, blk))
@@ -349,19 +352,25 @@
 
     def finish(j, h):
         d2d_in(j, h)
-        for n in range(h * per, (h + 1) * per):
+        tiles = range(h * per, (h + 1) * per)
+        for n in tiles:
             q[j - 1, n] = summed(j, n).astype(BF16)
-            send(j, n).start()
+        return lambda: [send(j, n).start() for n in tiles]
 
     def far_total(h):
         d2d_in(3, h)
         fold(jnp.concatenate([summed(3, n) for n in range(h * per, (h + 1) * per)], axis=1), snd2_o, h)
-        start_all(f_copies[h])
         ret_o[h, 0] = snd2_o[h, 0]
+        return lambda: start_all(f_copies[h])
 
     def down_pass(j):
         down_tiles(j, range(per))
         down_tiles(j, range(per, NT))
+
+    def other_side():
+        for h in range(2):
+            from_near(2, h)
+            pair[2][h].start()
 
     local[11].wait()
     local[12].wait()
@@ -371,15 +380,15 @@
         pair_in(0)
         gate_up(0)
 
-    from_near(1, 0)
-    pair[1][0].start()
-    from_near(1, 1)
-    pair[1][1].start()
     for is_first, copies in to_near:
         @pl.when(jnp.logical_not(is_first))
         def _():
             copies[0].start()
             copies[1].start()
+    from_near(1, 0)
+    pair[1][0].start()
+    from_near(1, 1)
+    pair[1][1].start()
     @pl.when(y != 0)
     def _():
         down_tiles(0, range(NT))
@@ -392,24 +401,26 @@
     gate_up(1)
     down_pass(1)
     pair_in(3)
-    gate_up(3, (None, lambda: finish(1, 0), lambda: finish(1, 1)))
-    for h in range(2):
-        from_near(2, h)
-        pair[2][h].start()
-    down_pass(3)
+    gate_up(3, {2: other_side, 3: lambda: finish(1, 0)})
+    down_tiles(3, range(per))
+    finish(1, 1)()
+    down_tiles(3, range(per, NT))
     pair_in(2)
-    gate_up(2, (None, lambda: far_total(0), lambda: far_total(1)))
+    gate_up(2)
     down_pass(2)
     @pl.when(y == 0)
     def _():
         pair_in(0)
-        gate_up(0, (None, lambda: finish(2, 0), lambda: finish(2, 1)))
+        gate_up(0, {
+            0: lambda: far_total(0), 1: lambda: finish(2, 0), 2: lambda: far_total(1), 3: lambda: finish(2, 1),
+        })
         down_pass(0)
 
     @pl.when(y != 0)
     def _():
-        finish(2, 0)
-        finish(2, 1)
+        for h in range(2):
+            far_total(h)()
+            finish(2, h)()
 
     def picked(place, weight, src, h):
         came = unfold(src, h)
@@ -437,11 +448,11 @@
         ret[h, 0] = snd2[h, 0]
 
     own_total(0)
+    own_total(1)
     for h in range(2):
         arrive_all(ret_o, f_r, h)
         part_o[:, h * half:(h + 1) * half] = picked(place_o, weight_o, ret_o, h).astype(BF16)
-    far_copies[4].start()
-    own_total(1)
+        far_copies[4 + h].start()
     halo_copy.wait_send()
 
     @pl.when(tp != 0)
@@ -462,10 +473,12 @@
         arrive_all(ret, e_r, h)
         acc[:, cols] = RESIDUAL * normed[:, cols].astype(F32) + picked(place, weight, ret, h)
     far_copies[4].wait_recv()
+    far_copies[5].wait_recv()
     acc[...] += part[...].astype(F32)
     out_ref[...] = layer_norm(acc[...], ng[1:2, :], nb[1:2, :]).astype(BF16)
 
     far_copies[4].wait_send()
+    far_copies[5].wait_send()
     whole(snd2.at[:, pl.ds(1, NSP - 1)], e_s)
 
 
@@ -524,7 +537,7 @@
         dma((14,)), dma, dma, dma, dma, dma, dma((NTP,)), dma, dma((2,)),
         dma, dma((4,)), dma, dma((4,)), dma, dma((8,)),
         dma, dma((4,)), dma, dma((2,)),
-        dma((5,)), dma((5,)), dma, dma((2,)), dma, dma((2,)),
+        dma((6,)), dma((6,)), dma, dma((2,)), dma, dma((2,)),
     ]
     return pl.pallas_call(
         body,

time: 49.6 us -> 47.8 us (0.964)
  Pallas kernels: 48.8 us -> 47.1 us
    pallas_call x1, Pallas kernels: 48.8 us -> 47.1 us  [shards(): pl.pallas_call(body, out_shape=jax.ShapeDtypeStruct((rows, model), BF16),...]
where the time goes in v4:
time: 47.8 us; the launch traced here: 47.7 us
  Pallas kernels  47.1 us (99%)
  local copies, waits for them, and re-layouts  0.66 us (1%)
    pallas_call x1, Pallas kernels, shards(): pl.pallas_call(body, out_shape=jax.ShapeDtypeStruct((rows, model), BF16),...  47.1 us

profile of v4, /device:TPU:0, one launch (start us, length us, event | category | flops | bytes accessed | tf_op | source)
XLA Modules:
  0.0 47.7 jit_solution(10489600211182656831)
XLA Ops:
  0.0 47.1 %layer.1 = bf16[32,2048]{1,0:T(8,128)(2,1)S(1)} custom-call(bf16[32,2048]{1,0:T(8,128)(2,1)} %stream_h.1, bf16[256,256]{1,0:T(8,128)(2,1)} %og_h.1, bf16[256,256]{1,0:T(8,128)(2,1)} %ig_h.1, bf16[256,256]{1,0:T(8,128)(2,1)} %va_h.1, f32[3,256]{1,0:T(4,128)} %cw_h.1, bf16[2048,2048]{1,0:T(8,128)(2,1)} %ow_h.1, s32[1,256]{1,0:T(1,128)} %bitcast.3, ...), custom_call_target="tpu_custom_call" | custom-call | tf_op jit(solution)/shard_map/layer/pallas_call | solution.py:542
  47.1 0.7 %copy.16 = bf16[32,2048]{1,0:T(8,128)(2,1)} copy(bf16[32,2048]{1,0:T(8,128)(2,1)S(1)} %layer.1) | data formatting | bytes 262144

commit v5 on v4

--- a/solution.py
+++ b/solution.py
@@ -187,10 +187,12 @@
         def _():
             remote(term, terms.at[tp], i_s, i_r, (sp, 0)).start()
 
-    edge_rows()
+    pl.when(x != 0)(edge_rows)
     for o in (1, 2, 3, 6, 7, 4, 5):
         a_copies[o - 1].wait_recv()
         acc[...] += project(tr[o], tp_from(o))
+        if o == 3:
+            pl.when(x == 0)(edge_rows)
     @pl.when(tp == 0)
     def _():
         whole(terms.at[pl.ds(1, NTP - 1)], i_r)
@@ -249,7 +251,7 @@
     far_copies[1].wait_recv()
     place_o = placed(rt_o)
     def side_of(row):
-        return (1 - 2 * c) * (1 - 2 * (row // 3))
+        return (1 - 2 * c) * (2 * (((row + 1) % 4) // 2) - 1)
 
     side = side_of(y)
     above, below = (y + 1) % 4, (y + 3) % 4
@@ -407,20 +409,18 @@
     down_tiles(3, range(per, NT))
     pair_in(2)
     gate_up(2)
-    down_pass(2)
+    down_tiles(2, range(per))
+    far_total(0)()
+    down_tiles(2, range(per, NT))
+    finish(2, 0)()
+    far_total(1)()
+    finish(2, 1)()
+
     @pl.when(y == 0)
     def _():
         pair_in(0)
-        gate_up(0, {
-            0: lambda: far_total(0), 1: lambda: finish(2, 0), 2: lambda: far_total(1), 3: lambda: finish(2, 1),
-        })
+        gate_up(0)
         down_pass(0)
-
-    @pl.when(y != 0)
-    def _():
-        for h in range(2):
-            far_total(h)()
-            finish(2, h)()
 
     def picked(place, weight, src, h):
         came = unfold(src, h)
@@ -447,12 +447,15 @@
         start_all(e_copies[h])
         ret[h, 0] = snd2[h, 0]
 
-    own_total(0)
-    own_total(1)
-    for h in range(2):
+    def far_part(h):
         arrive_all(ret_o, f_r, h)
         part_o[:, h * half:(h + 1) * half] = picked(place_o, weight_o, ret_o, h).astype(BF16)
         far_copies[4 + h].start()
+
+    own_total(0)
+    far_part(0)
+    own_total(1)
+    far_part(1)
     halo_copy.wait_send()
 
     @pl.when(tp != 0)

time: 47.8 us -> 48 us (level)
  no operation moved by 1% of the time
where the time goes in v5:
time: 48 us; the launch traced here: 47.7 us
  Pallas kernels  47 us (98%)
  local copies, waits for them, and re-layouts  0.66 us (1%)
    pallas_call x1, Pallas kernels, shards(): pl.pallas_call(body, out_shape=jax.ShapeDtypeStruct((rows, model), BF16),...  47 us

profile of v5, /device:TPU:0, one launch (start us, length us, event | category | flops | bytes accessed | tf_op | source)
XLA Modules:
  0.0 47.7 jit_solution(13971198675447390105)
XLA Ops:
  0.0 47.0 %layer.1 = bf16[32,2048]{1,0:T(8,128)(2,1)S(1)} custom-call(bf16[32,2048]{1,0:T(8,128)(2,1)} %stream_h.1, bf16[256,256]{1,0:T(8,128)(2,1)} %og_h.1, bf16[256,256]{1,0:T(8,128)(2,1)} %ig_h.1, bf16[256,256]{1,0:T(8,128)(2,1)} %va_h.1, f32[3,256]{1,0:T(4,128)} %cw_h.1, bf16[2048,2048]{1,0:T(8,128)(2,1)} %ow_h.1, s32[1,256]{1,0:T(1,128)} %bitcast.3, ...), custom_call_target="tpu_custom_call" | custom-call | tf_op jit(solution)/shard_map/layer/pallas_call | solution.py:545
  47.0 0.7 %copy.16 = bf16[32,2048]{1,0:T(8,128)(2,1)} copy(bf16[32,2048]{1,0:T(8,128)(2,1)S(1)} %layer.1) | data formatting | bytes 262144

commit v6 on v5

--- a/solution.py
+++ b/solution.py
@@ -389,12 +389,12 @@
             copies[1].start()
     from_near(1, 0)
     pair[1][0].start()
-    from_near(1, 1)
-    pair[1][1].start()
     @pl.when(y != 0)
     def _():
         down_tiles(0, range(NT))
 
+    from_near(1, 1)
+    pair[1][1].start()
     for h in range(2):
         arrive_all(rcv_o, c_r, h)
         settle(rcv_o, 3, h)

time: 48 us -> 48 us (level)
  no operation moved by 1% of the time
where the time goes in v6:
time: 48 us; the launch traced here: 47.7 us
  Pallas kernels  47 us (98%)
  local copies, waits for them, and re-layouts  0.66 us (1%)
    pallas_call x1, Pallas kernels, shards(): pl.pallas_call(body, out_shape=jax.ShapeDtypeStruct((rows, model), BF16),...  47 us

profile of v6, /device:TPU:0, one launch (start us, length us, event | category | flops | bytes accessed | tf_op | source)
XLA Modules:
  0.0 47.7 jit_solution(13647805621449343976)
XLA Ops:
  0.0 47.0 %layer.1 = bf16[32,2048]{1,0:T(8,128)(2,1)S(1)} custom-call(bf16[32,2048]{1,0:T(8,128)(2,1)} %stream_h.1, bf16[256,256]{1,0:T(8,128)(2,1)} %og_h.1, bf16[256,256]{1,0:T(8,128)(2,1)} %ig_h.1, bf16[256,256]{1,0:T(8,128)(2,1)} %va_h.1, f32[3,256]{1,0:T(4,128)} %cw_h.1, bf16[2048,2048]{1,0:T(8,128)(2,1)} %ow_h.1, s32[1,256]{1,0:T(1,128)} %bitcast.3, ...), custom_call_target="tpu_custom_call" | custom-call | tf_op jit(solution)/shard_map/layer/pallas_call | solution.py:545
  47.0 0.7 %copy.16 = bf16[32,2048]{1,0:T(8,128)(2,1)} copy(bf16[32,2048]{1,0:T(8,128)(2,1)S(1)} %layer.1) | data formatting | bytes 262144
